TPU v7x, 128 devices: a whole 4x4x4 slice. The times are simulated.
128 devices in a mesh: kv: 16 (over z, x), tp: 8 (over y, core).
Axes of the slice: x: 4, y: 4, z: 4, core: 2. Of those that a mesh axis runs over, the one named last changes fastest.
Arguments:
- tokens: bfloat16 [96, 4096], P(None, 'kv'), may hold values from -210 to 210
- norm_gain: float32 [4096], P('kv'), may hold values from 0.1 to 1.9
- w_query: bfloat16 [4096, 4096], P('kv', 'tp'), may hold values from -1 to 1
- w_key: bfloat16 [4096, 4096], P('kv', 'tp'), may hold values from -2 to 2
- w_value: bfloat16 [4096, 4096], P('kv', 'tp'), may hold values from -0.09375 to 0.09375
- w_output: bfloat16 [4096, 4096], P('tp', 'kv'), may hold values from -0.09375 to 0.09375
- cache_keys: bfloat16 [4, 8192, 4096], P(None, 'kv', 'tp'), may hold values from -820 to 820
- cache_values: bfloat16 [4, 8192, 4096], P(None, 'kv', 'tp'), may hold values from -6 to 6
- map_lambda: float32 [64], P('tp'), may hold values from 0.3 to 0.8
- out_gain: float32 [4096], P('tp'), may hold values from 0.1 to 1.9
- parents: int32 [4, 24], replicated, may hold values from -1 to 22, as said below
- lengths: int32 [4], replicated, may hold values from 4096 to 8144, as said below
- accepted: int32 [4], replicated, may hold values from 0 to 24
Outputs:
- mixed: bfloat16 [96, 4096], P(None, 'kv')
- new_keys: bfloat16 [4, 8192, 4096], P(None, 'kv', 'tp')
- new_values: bfloat16 [4, 8192, 4096], P(None, 'kv', 'tp')
Inputs may be any that keep to these rules, and one draw needn't show every extreme that they name: parents[b, j] lies between -1 and j - 1. `lengths`: some sequence has exactly the largest value.
All inputs are finite; a program needn't handle non-finite values.
Results may differ from a plain program's by a relative error of at most 0.029.
Values may be sent and summed in bfloat16 or wider, within the bound.
No kernel may reach another device: no remote copies, remote signals or barrier semaphores. Data moves between devices by JAX's collectives and lax.ppermute only.
A program may use at most 128 MiB of HBM per device.

v0:
```python
import functools

import jax
import jax.numpy as jnp
from jax import lax
from jax.sharding import Mesh
from jax.sharding import PartitionSpec as P

D = 4096
HEAD = 64
QK = 32
SEQS = 4
PROP = 24
KV = ("kv_0", "kv_1")


epsilon = 1e-05
masked_low = -1e30


def over_axes(array, axes):
    return functools.reduce(lax.psum, axes, array)


def cut_along(array, dim, length):
    lengths = array.shape
    blocks = array.reshape(*lengths[:dim], length, lengths[dim] // length, *lengths[dim + 1 :])
    return jnp.moveaxis(blocks, dim, 0)


def sum_at_owner(array, axis, dim):
    blocks = cut_along(array, dim, lax.axis_size(axis))
    arrived = lax.all_to_all(blocks, axis, split_axis=0, concat_axis=0, tiled=True)
    return arrived.sum(axis=0)


def in_order(blocks, dim):
    blocks = jnp.moveaxis(blocks, 0, dim)
    lengths = blocks.shape
    return blocks.reshape(*lengths[:dim], lengths[dim] * lengths[dim + 1], *lengths[dim + 2 :])


def copy_for_each(array, axis):
    copies = jnp.broadcast_to(array, (lax.axis_size(axis), *array.shape))
    return lax.all_to_all(copies, axis, split_axis=0, concat_axis=0, tiled=True)


def gathered_copies(array, axis, dim):
    return in_order(copy_for_each(array, axis), dim)


def folded_in_pairs(pieces, combine):
    while len(jax.tree.leaves(pieces)[0]) > 1:
        pieces = jax.vmap(combine)(
            *(jax.tree.map(lambda part: part[side::2], pieces) for side in (0, 1))
        )
    return jax.tree.map(lambda part: part[0], pieces)


def combined_all(array, axis, combine):
    pieces = jax.tree.map(
        lambda part: copy_for_each(part, axis),
        jax.tree.map(
            lambda part, kind: part.astype(kind), array, (jnp.bfloat16, jnp.bfloat16, jnp.bfloat16)
        ),
    )
    return folded_in_pairs(
        jax.tree.map(lambda part, own: part.astype(own.dtype), pieces, array), combine
    )


def over_copies(array, axis):
    return copy_for_each(array, axis).astype(jnp.float32).sum(axis=0)


def ancestry(parents):
    count = parents.shape[1]
    places = jnp.arange(count, dtype=jnp.int32)
    parent_links = (parents[:, :, None] == places[None, None, :]).astype(jnp.float32)
    identity = jnp.eye(count, dtype=jnp.float32)[None]

    def extend(turn_index, reached):
        return jnp.minimum(1.0, identity + jnp.einsum("bji,bik->bjk", parent_links, reached))

    reached = lax.fori_loop(0, count, extend, jnp.broadcast_to(identity, parent_links.shape))
    return reached > 0.5


def scaled_values(values, factor, local_heads):
    shaped = values.astype(jnp.float32).reshape(values.shape[0], 2, PROP, local_heads, HEAD)
    return shaped * jnp.transpose(factor, (0, 1, 3, 2))[..., None]


def combine_blocks(earlier, later):
    max_first, total_first, values_first = earlier
    max_second, total_second, values_second = later
    largest = jnp.maximum(max_first, max_second)
    factor_first = jnp.exp(max_first - largest)
    factor_second = jnp.exp(max_second - largest)
    summed_total = total_first * factor_first + total_second * factor_second
    local_heads = max_first.shape[2]
    merged = scaled_values(values_first, factor_first, local_heads) + scaled_values(
        values_second, factor_second, local_heads
    )
    merged = merged.reshape(values_first.shape).astype(jnp.bfloat16)
    return (largest, summed_total, merged)


def local(
    tokens,
    norm_gain,
    w_query,
    w_key,
    w_value,
    w_output,
    cache_keys,
    cache_values,
    map_lambda,
    out_gain,
    parents,
    lengths,
    accepted,
):
    f32 = jnp.float32
    bf16 = jnp.bfloat16
    tokens_wide = tokens.astype(f32)
    gained = (tokens_wide * norm_gain).astype(bf16)
    partial_value = jnp.concatenate(
        [
            jnp.dot(gained, weight_part, preferred_element_type=f32)
            for weight_part in (w_query, w_key, w_value)
        ],
        axis=1,
    )
    squares = jnp.sum(tokens_wide * tokens_wide, axis=1)
    total_squares = over_axes(squares, KV)
    norm_factor = lax.rsqrt(total_squares / D + epsilon)
    share = sum_at_owner(partial_value, KV, 1)
    projected = gathered_copies((share * norm_factor[:, None]).astype(bf16), KV, 1)
    width = w_query.shape[1]
    local_heads = width // HEAD
    queries = projected[:, :width].reshape(SEQS, PROP, local_heads, 2, QK)
    keys_flat = projected[:, width : 2 * width].reshape(SEQS, PROP, width)
    values_flat = projected[:, 2 * width :].reshape(SEQS, PROP, width)
    keys_new = keys_flat.reshape(SEQS, PROP, local_heads, 2, QK)
    values_new = values_flat.reshape(SEQS, PROP, local_heads, HEAD)
    start = lengths + accepted
    score_scale = QK ** (-0.5)
    block_len = cache_keys.shape[1]
    offset = lax.axis_index(KV) * block_len
    positions = offset + jnp.arange(block_len, dtype=jnp.int32)
    visible = (positions[None, :] < start[:, None])[:, None, None, None, :]
    block_keys = cache_keys.reshape(SEQS, block_len, local_heads, 2, QK)
    block_vals = cache_values.reshape(SEQS, block_len, local_heads, HEAD)
    scores = (
        jnp.einsum("bqhmd,bkhmd->bmhqk", queries, block_keys, preferred_element_type=f32)
        * score_scale
    )
    block_max = jnp.max(jnp.where(visible, scores, masked_low), axis=-1)
    block_weight = jnp.where(visible, jnp.exp(scores - block_max[..., None]), 0.0)
    block_total = jnp.sum(block_weight, axis=-1)
    block_values = jnp.einsum(
        "bmhqk,bkhd->bmqhd", block_weight.astype(bf16), block_vals, preferred_element_type=f32
    )
    block_values = block_values.reshape(SEQS, 2, PROP, width).astype(bf16)
    cache_max, cache_total, cache_sum = combined_all(
        (block_max, block_total, block_values), KV, combine_blocks
    )
    lineage = ancestry(parents)[:, None, None, :, :]
    self_scores = (
        jnp.einsum("bqhmd,bjhmd->bmhqj", queries, keys_new, preferred_element_type=f32)
        * score_scale
    )
    self_max = jnp.max(jnp.where(lineage, self_scores, masked_low), axis=-1)
    top = jnp.maximum(cache_max, self_max)
    self_weight = jnp.where(lineage, jnp.exp(self_scores - top[..., None]), 0.0)
    carried = jnp.exp(cache_max - top)
    denominator = cache_total * carried + jnp.sum(self_weight, axis=-1)
    self_values = jnp.einsum(
        "bmhqj,bjhd->bmqhd", self_weight.astype(bf16), values_new, preferred_element_type=f32
    )
    attended = (scaled_values(cache_sum, carried, local_heads) + self_values) / jnp.transpose(
        denominator, (0, 1, 3, 2)
    )[..., None]
    difference = attended[:, 0] - map_lambda[None, None, :, None] * attended[:, 1]
    gains = out_gain.reshape(local_heads, HEAD)[None, None]
    normed = (
        difference
        * lax.rsqrt(jnp.mean(difference * difference, axis=-1, keepdims=True) + epsilon)
        * gains
    )
    normed = normed.astype(bf16).reshape(SEQS * PROP, width)
    partial_out = jnp.dot(normed, w_output, preferred_element_type=f32).astype(bf16)
    partial_out = lax.optimization_barrier(partial_out).astype(f32)
    mixed = over_copies(partial_out.astype(jnp.bfloat16), "tp").astype(jnp.float32).astype(bf16)
    relative = positions[None, :] - start[:, None]
    slots = jnp.arange(PROP, dtype=jnp.int32)
    placing = (relative[:, :, None] == slots[None, None, :]).astype(bf16)
    written = ((relative >= 0) & (relative < PROP))[:, :, None]
    moved_keys = jnp.einsum("bkj,bjf->bkf", placing, keys_flat, preferred_element_type=f32).astype(
        bf16
    )
    moved_values = jnp.einsum(
        "bkj,bjf->bkf", placing, values_flat, preferred_element_type=f32
    ).astype(bf16)
    new_keys = jnp.where(written, moved_keys, cache_keys)
    new_values = jnp.where(written, moved_values, cache_values)
    return (mixed, new_keys, new_values)


def solution(mesh):
    torus = Mesh(mesh.devices.reshape(4, 4, mesh.shape["tp"]), ("kv_0", "kv_1", "tp"))
    return jax.shard_map(
        local,
        mesh=torus,
        in_specs=(
            P(None, KV),
            P(KV),
            P(KV, "tp"),
            P(KV, "tp"),
            P(KV, "tp"),
            P("tp", KV),
            P(None, KV, "tp"),
            P(None, KV, "tp"),
            P("tp"),
            P("tp"),
            P(),
            P(),
            P(),
        ),
        out_specs=(P(None, KV), P(None, KV, "tp"), P(None, KV, "tp")),
        check_vma=False,
    )
```

profile of v0, /device:TPU:1, one launch (start us, length us, event | category | flops | bytes accessed | tf_op | source)
XLA Modules:
  0.0 160.8 jit_solution(7291358375823799381)
XLA Ops:
  6.4 8.4 %all-to-all-start = ((f32[16,96,96]{2,1,0:T(8,128)}), f32[16,96,96]{2,1,0:T(8,128)S(1)}, u32[]{:S(2)}, u32[]{:S(2)}) async-start(f32[16,96,96]{2,1,0:T(8,128)} %bitcast.118), calls=%async_computation | async-start | bytes 1572864 | tf_op jit(solution)/shard_map/all_to_all | solution.py:33
  14.8 5.8 %while.11 = (s32[]{:T(128)}, f32[4,24,24]{2,1,0:T(8,128)S(1)}, s32[4,24]{1,0:T(4,128)S(1)}, s32[]{:T(128)}) while((s32[]{:T(128)}, f32[4,24,24]{2,1,0:T(8,128)S(1)}, s32[4,24]{1,0:T(4,128)S(1)}, s32[]{:T(128)}) %tuple.46), condition=%wide.region_6.7_spmd.clone, body=%wide.region_5.6_spmd.clone.sunk | while | flops 120962 | bytes 41909 | solution.py:85
  20.7 9.4 %psum.14 = f32[96]{0:T(128)S(1)} all-reduce(f32[96]{0:T(128)S(1)} %fusion.38), channel_id=1, replica_groups=mesh['kv_0'=4,'kv_1'=4,'tp'=8] {'kv_0'}, use_global_device_ids=true, to_apply=%region_2.0 | all-reduce | flops 96 | bytes 768 | tf_op jit(solution)/shard_map/psum | solution.py:22
  30.1 7.7 %psum.15 = f32[96]{0:T(128)S(1)} all-reduce(f32[96]{0:T(128)S(1)} %psum.14), channel_id=1, replica_groups=mesh['kv_0'=4,'kv_1'=4,'tp'=8] {'kv_1'}, use_global_device_ids=true, to_apply=%region_3.0 | all-reduce | flops 96 | bytes 768 | tf_op jit(solution)/shard_map/psum | solution.py:22
  38.8 3.6 %all-to-all-start.1 = ((bf16[16,96,96]{2,1,0:T(8,128)(2,1)}), bf16[16,96,96]{2,1,0:T(8,128)(2,1)S(1)}, u32[]{:S(2)}, u32[]{:S(2)}) async-start(bf16[16,96,96]{2,1,0:T(8,128)(2,1)} %broadcast_in_dim.96), calls=%async_computation.1 | async-start | bytes 786432 | tf_op jit(solution)/shard_map/all_to_all | solution.py:45
  42.4 2.8 %copy.114 = bf16[4,512,512]{1,2,0:T(8,128)(2,1)S(1)} copy(bf16[4,512,512]{2,1,0:T(8,128)(2,1)} %param.21) | data formatting | bytes 4194304 | tf_op args[6]
  45.3 5.3 %all-to-all-done.1 = bf16[16,96,96]{2,1,0:T(8,128)(2,1)S(1)} async-done(((bf16[16,96,96]{2,1,0:T(8,128)(2,1)}), bf16[16,96,96]{2,1,0:T(8,128)(2,1)S(1)}, u32[]{:S(2)}, u32[]{:S(2)}) %all-to-all-start.1) | async-done | bytes 294944 | tf_op jit(solution)/shard_map/all_to_all | solution.py:45
  52.3 2.2 %fusion.67 = (bf16[4,2,8,24,512]{4,3,2,1,0:T(8,128)(2,1)}, bf16[4,2,8,24]{3,2,1,0:T(8,128)(2,1)S(1)}) fusion(f32[4,2,8,24,512]{4,3,2,1,0:T(8,128)S(1)} %get-tuple-element.73, pred[4,512]{1,0:T(4,128)(4,1)S(1)} %get-tuple-element.68), kind=kOutput, calls=%fused_computation.111 | output fusion | flops 5505535 | bytes 4723712 | tf_op jit(solution)/shard_map/sub | solution.py:160
  55.6 3.5 %all-to-all-start.4 = ((bf16[16,2,768]{2,1,0:T(2,128)(2,1)}), bf16[16,2,768]{2,1,0:T(2,128)(2,1)S(1)}, u32[]{:S(2)}, u32[]{:S(2)}) async-start(bf16[16,2,768]{2,1,0:T(2,128)(2,1)} %reshape.218), calls=%async_computation.4 | async-start | bytes 98304 | tf_op jit(solution)/shard_map/all_to_all | solution.py:45
  59.1 2.4 %copy.117 = bf16[4,512,512]{1,2,0:T(8,128)(2,1)} copy(bf16[4,512,512]{2,1,0:T(8,128)(2,1)S(1)} %copy-done.3) | data formatting | bytes 4194304 | tf_op args[7]
  62.5 3.0 %all-to-all-done.4 = bf16[16,2,768]{2,1,0:T(2,128)(2,1)S(1)} async-done(((bf16[16,2,768]{2,1,0:T(2,128)(2,1)}), bf16[16,2,768]{2,1,0:T(2,128)(2,1)S(1)}, u32[]{:S(2)}, u32[]{:S(2)}) %all-to-all-start.4) | async-done | bytes 49184 | tf_op jit(solution)/shard_map/all_to_all | solution.py:45
  65.5 3.6 %all-to-all-start.3 = ((bf16[16,2,768]{2,1,0:T(2,128)(2,1)}), bf16[16,2,768]{2,1,0:T(2,128)(2,1)S(1)}, u32[]{:S(2)}, u32[]{:S(2)}) async-start(bf16[16,2,768]{2,1,0:T(2,128)(2,1)} %reshape.216), calls=%async_computation.3 | async-start | bytes 98304 | tf_op jit(solution)/shard_map/all_to_all | solution.py:45
  69.1 2.8 %fusion.24 = bf16[4,2,24,8,64]{4,2,1,3,0:T(8,128)(2,1)S(1)} fusion(bf16[4,512,8,64,1]{1,3,4,2,0:T(8,128)(2,1)} %bitcast.124, bf16[4,2,8,24,512]{4,3,2,1,0:T(8,128)(2,1)} %get-tuple-element.50), kind=kOutput, calls=%fused_computation.30 | convolution fusion | flops 100761600 | bytes 3866624 | tf_op jit(solution)/shard_map/bmhqk,bkhd->bmqhd/dot_general | solution.py:162
  72.3 3.3 %all-to-all-done.3 = bf16[16,2,768]{2,1,0:T(2,128)(2,1)S(1)} async-done(((bf16[16,2,768]{2,1,0:T(2,128)(2,1)}), bf16[16,2,768]{2,1,0:T(2,128)(2,1)S(1)}, u32[]{:S(2)}, u32[]{:S(2)}) %all-to-all-start.3) | async-done | bytes 49184 | tf_op jit(solution)/shard_map/all_to_all | solution.py:45
  77.6 4.8 %all-to-all-start.2 = ((bf16[16,4,2,24,512]{4,3,2,1,0:T(8,128)(2,1)}), bf16[16,4,2,24,512]{4,3,2,1,0:T(8,128)(2,1)}, u32[]{:S(2)}, u32[]{:S(2)}) async-start(bf16[16,4,2,24,512]{4,3,2,1,0:T(8,128)(2,1)} %broadcast_in_dim.99), calls=%async_computation.2 | async-start | bytes 6291456 | tf_op jit(solution)/shard_map/all_to_all | solution.py:45
  87.9 3.8 %mul.219 = f32[8,4,2,24,8,64]{5,4,3,2,1,0:T(8,128)} broadcast(f32[8,4,2,24,8]{4,3,2,1,0:T(8,128)S(1)} %copy.120), dimensions={0,1,2,3,4} | broadcast | bytes 3194880 | tf_op jit(solution)/shard_map/vmap()/mul | solution.py:91
  91.8 6.3 %mul.220 = f32[8,4,2,24,512]{4,3,2,1,0:T(8,128)} reshape(f32[8,4,2,24,8,64]{5,4,3,2,1,0:T(8,128)} %mul.219) | data formatting | bytes 6291456 | tf_op jit(solution)/shard_map/vmap()/mul | solution.py:91
  98.3 3.8 %mul.222 = f32[8,4,2,24,8,64]{5,4,3,2,1,0:T(8,128)} broadcast(f32[8,4,2,24,8]{4,3,2,1,0:T(8,128)S(1)} %copy.121), dimensions={0,1,2,3,4} | broadcast | bytes 3194880 | tf_op jit(solution)/shard_map/vmap()/mul | solution.py:91
  102.1 6.2 %mul.223 = f32[8,4,2,24,512]{4,3,2,1,0:T(8,128)} reshape(f32[8,4,2,24,8,64]{5,4,3,2,1,0:T(8,128)} %mul.222) | data formatting | bytes 6291456 | tf_op jit(solution)/shard_map/vmap()/mul | solution.py:91
  123.1 2.2 %mul.239 = f32[1,4,2,24,512]{4,3,2,1,0:T(8,128)} reshape(f32[4,2,24,8,64]{4,3,2,1,0:T(8,128)} %mul.238) | data formatting | bytes 786432 | tf_op jit(solution)/shard_map/vmap()/mul | solution.py:91
  126.6 2.1 %mul.243 = f32[1,4,2,24,512]{4,3,2,1,0:T(8,128)} reshape(f32[4,2,24,8,64]{4,3,2,1,0:T(8,128)} %mul.242) | data formatting | bytes 786432 | tf_op jit(solution)/shard_map/vmap()/mul | solution.py:91
  128.7 4.1 %add_convert_fusion = bf16[8,4,2,24,512]{4,3,2,1,0:T(8,128)(2,1)S(1)} fusion(f32[8,4,2,24,512]{4,3,2,1,0:T(8,128)} %mul.223, f32[8,4,2,24,512]{4,3,2,1,0:T(8,128)S(1)} %copy-done.2, bf16[16,4,2,24,512]{4,3,2,1,0:T(8,128)(2,1)} %all-to-all-done.2), kind=kLoop, calls=%fused_computation.10 | loop fusion | flops 4718592 | bytes 11010048 | tf_op jit(solution)/shard_map/vmap()/convert_element_type | solution.py:105
  139.6 12.8 %all-to-all-start.5 = ((bf16[8,96,256]{2,1,0:T(8,128)(2,1)}), bf16[8,96,256]{2,1,0:T(8,128)(2,1)S(1)}, u32[]{:S(2)}, u32[]{:S(2)}) async-start(bf16[8,96,256]{2,1,0:T(8,128)(2,1)} %broadcast_in_dim.106), calls=%async_computation.5 | async-start | bytes 786432 | tf_op jit(solution)/shard_map/all_to_all | solution.py:45
  156.4 3.7 %all-to-all-done.5 = bf16[8,96,256]{2,1,0:T(8,128)(2,1)S(1)} async-done(((bf16[8,96,256]{2,1,0:T(8,128)(2,1)}), bf16[8,96,256]{2,1,0:T(8,128)(2,1)S(1)}, u32[]{:S(2)}, u32[]{:S(2)}) %all-to-all-start.5) | async-done | bytes 393248 | tf_op jit(solution)/shard_map/all_to_all | solution.py:45
  (229 shorter events, 51.2 us)
Async XLA Ops:
  5.0 9.9 %copy-start.25 = (s32[4,24]{1,0:T(4,128)S(1)}, s32[4,24]{1,0:T(4,128)}, u32[]{:S(2)}) copy-start(s32[4,24]{1,0:T(4,128)} %param.25) | copy-start | bytes 1156
  5.2 15.4 %copy-start.18 = (bf16[96,256]{1,0:T(8,128)(2,1)S(1)}, bf16[96,256]{1,0:T(8,128)(2,1)}, u32[]{:S(2)}) copy-start(bf16[96,256]{1,0:T(8,128)(2,1)} %param.15) | copy-start | bytes 147460
  6.4 31.5 %all-to-all-start = ((f32[16,96,96]{2,1,0:T(8,128)}), f32[16,96,96]{2,1,0:T(8,128)S(1)}, u32[]{:S(2)}, u32[]{:S(2)}) async-start(f32[16,96,96]{2,1,0:T(8,128)} %bitcast.118), calls=%async_computation | async-start | bytes 1572864 | tf_op jit(solution)/shard_map/all_to_all | solution.py:33
  38.8 11.8 %all-to-all-start.1 = ((bf16[16,96,96]{2,1,0:T(8,128)(2,1)}), bf16[16,96,96]{2,1,0:T(8,128)(2,1)S(1)}, u32[]{:S(2)}, u32[]{:S(2)}) async-start(bf16[16,96,96]{2,1,0:T(8,128)(2,1)} %broadcast_in_dim.96), calls=%async_computation.1 | async-start | bytes 786432 | tf_op jit(solution)/shard_map/all_to_all | solution.py:45
  42.4 2.8 %copy-start.30 = (s32[4]{0:T(128)S(1)}, s32[4]{0:T(128)}, u32[]{:S(2)}) copy-start(s32[4]{0:T(128)} %param.26) | copy-start | bytes 52
  42.4 2.8 %copy-start.31 = (s32[4]{0:T(128)S(1)}, s32[4]{0:T(128)}, u32[]{:S(2)}) copy-start(s32[4]{0:T(128)} %param.27) | copy-start | bytes 52
  51.2 31.6 %copy-start.16 = (bf16[96,512]{1,0:T(8,128)(2,1)}, bf16[96,512]{1,0:T(8,128)(2,1)S(1)}, u32[]{:S(2)}) copy-start(bf16[96,512]{1,0:T(8,128)(2,1)S(1)} %get-tuple-element.61) | copy-start | bytes 294916
  51.2 31.8 %copy-start.14 = (bf16[96,512]{1,0:T(8,128)(2,1)}, bf16[96,512]{1,0:T(8,128)(2,1)S(1)}, u32[]{:S(2)}) copy-start(bf16[96,512]{1,0:T(8,128)(2,1)S(1)} %get-tuple-element.60) | copy-start | bytes 294916
  52.3 6.8 %copy-start.3 = (bf16[4,512,512]{2,1,0:T(8,128)(2,1)S(1)}, bf16[4,512,512]{2,1,0:T(8,128)(2,1)}, u32[]{:S(2)}) copy-start(bf16[4,512,512]{2,1,0:T(8,128)(2,1)} %param.22) | copy-start | bytes 6291460
  55.6 9.9 %all-to-all-start.4 = ((bf16[16,2,768]{2,1,0:T(2,128)(2,1)}), bf16[16,2,768]{2,1,0:T(2,128)(2,1)S(1)}, u32[]{:S(2)}, u32[]{:S(2)}) async-start(bf16[16,2,768]{2,1,0:T(2,128)(2,1)} %reshape.218), calls=%async_computation.4 | async-start | bytes 98304 | tf_op jit(solution)/shard_map/all_to_all | solution.py:45
  65.5 10.1 %all-to-all-start.3 = ((bf16[16,2,768]{2,1,0:T(2,128)(2,1)}), bf16[16,2,768]{2,1,0:T(2,128)(2,1)S(1)}, u32[]{:S(2)}, u32[]{:S(2)}) async-start(bf16[16,2,768]{2,1,0:T(2,128)(2,1)} %reshape.216), calls=%async_computation.3 | async-start | bytes 98304 | tf_op jit(solution)/shard_map/all_to_all | solution.py:45
  77.6 5.0 %copy-start.28 = (f32[8]{0:T(128)S(1)}, f32[8]{0:T(128)}, u32[]{:S(2)}) copy-start(f32[8]{0:T(128)} %param.23) | copy-start | bytes 100
  77.6 51.1 %all-to-all-start.2 = ((bf16[16,4,2,24,512]{4,3,2,1,0:T(8,128)(2,1)}), bf16[16,4,2,24,512]{4,3,2,1,0:T(8,128)(2,1)}, u32[]{:S(2)}, u32[]{:S(2)}) async-start(bf16[16,4,2,24,512]{4,3,2,1,0:T(8,128)(2,1)} %broadcast_in_dim.99), calls=%async_computation.2 | async-start | bytes 6291456 | tf_op jit(solution)/shard_map/all_to_all | solution.py:45
  85.3 2.4 %copy-start.10 = (f32[2,4,2,8,24]{4,3,2,1,0:T(8,128)}, f32[2,4,2,8,24]{4,3,2,1,0:T(8,128)S(1)}, u32[]{:S(2)}) copy-start(f32[2,4,2,8,24]{4,3,2,1,0:T(8,128)S(1)} %get-tuple-element.45) | copy-start | bytes 36868
  85.9 5.8 %copy-start.20 = (f32[1,4,2,8,24]{4,3,2,1,0:T(8,128)}, f32[1,4,2,8,24]{4,3,2,1,0:T(8,128)S(1)}, u32[]{:S(2)}) copy-start(f32[1,4,2,8,24]{4,3,2,1,0:T(8,128)S(1)} %get-tuple-element.43) | copy-start | bytes 18436
  121.9 6.7 %copy-start.24 = (f32[4,2,24,8]{2,3,1,0:T(8,128)S(1)}, f32[4,2,24,8]{2,3,1,0:T(8,128)}, u32[]{:S(2)}) copy-start(f32[4,2,24,8]{2,3,1,0:T(8,128)} %get-tuple-element.42) | copy-start | bytes 18436
  122.0 6.7 %copy-start.2 = (f32[8,4,2,24,512]{4,3,2,1,0:T(8,128)S(1)}, f32[8,4,2,24,512]{4,3,2,1,0:T(8,128)}, u32[]{:S(2)}) copy-start(f32[8,4,2,24,512]{4,3,2,1,0:T(8,128)} %mul.220) | copy-start | bytes 9437188
  128.7 4.1 %copy-start.6 = (f32[4,4,2,24,512]{4,3,2,1,0:T(8,128)S(1)}, f32[4,4,2,24,512]{4,3,2,1,0:T(8,128)}, u32[]{:S(2)}) copy-start(f32[4,4,2,24,512]{4,3,2,1,0:T(8,128)} %mul.226) | copy-start | bytes 4718596
  128.7 4.1 %copy-start.7 = (f32[4,4,2,24,512]{4,3,2,1,0:T(8,128)S(1)}, f32[4,4,2,24,512]{4,3,2,1,0:T(8,128)}, u32[]{:S(2)}) copy-start(f32[4,4,2,24,512]{4,3,2,1,0:T(8,128)} %mul.229) | copy-start | bytes 4718596
  137.1 15.3 %copy-start.4 = (bf16[4,512,512]{2,1,0:T(8,128)(2,1)S(1)}, bf16[4,512,512]{2,1,0:T(8,128)(2,1)}, u32[]{:S(2)}) copy-start(bf16[4,512,512]{2,1,0:T(8,128)(2,1)} %param.22) | copy-start | bytes 6291460
  137.1 15.3 %copy-start.15 = (bf16[96,512]{1,0:T(8,128)(2,1)S(1)}, bf16[96,512]{1,0:T(8,128)(2,1)}, u32[]{:S(2)}) copy-start(bf16[96,512]{1,0:T(8,128)(2,1)} %copy-done.14) | copy-start | bytes 294916
  139.6 20.5 %all-to-all-start.5 = ((bf16[8,96,256]{2,1,0:T(8,128)(2,1)}), bf16[8,96,256]{2,1,0:T(8,128)(2,1)S(1)}, u32[]{:S(2)}, u32[]{:S(2)}) async-start(bf16[8,96,256]{2,1,0:T(8,128)(2,1)} %broadcast_in_dim.106), calls=%async_computation.5 | async-start | bytes 786432 | tf_op jit(solution)/shard_map/all_to_all | solution.py:45
  152.4 2.0 %copy-start.5 = (bf16[4,512,512]{2,1,0:T(8,128)(2,1)S(1)}, bf16[4,512,512]{2,1,0:T(8,128)(2,1)}, u32[]{:S(2)}) copy-start(bf16[4,512,512]{2,1,0:T(8,128)(2,1)} %param.21) | copy-start | bytes 6291460
  154.4 6.4 %copy-start.1 = (bf16[256,512]{1,0:T(8,128)(2,1)S(1)}, bf16[256,512]{1,0:T(8,128)(2,1)}, u32[]{:S(2)}) copy-start(bf16[256,512]{1,0:T(8,128)(2,1)} %param.19) | copy-start | bytes 786436
  (14 other events, 18.6 us)
where the time goes:
time: 162 us; the launch traced here: 161 us
  local copies, waits for them, and re-layouts  60 us (37%)
  starting transfers between devices  36.6 us (23%)
  matrix products  18.4 us (11%)
  blocking collectives  17.2 us (11%)
  waiting for transfers between devices  15.2 us (9%)
  other arithmetic  11.5 us (7%)
    mul x18, local copies, waits for them, and re-layouts, scaled_values(): return shaped * jnp.transpose(factor, (0, 1, 3, 2))[..., None]  37.5 us
    all_to_all x5, starting transfers between devices, copy_for_each(): return lax.all_to_all(copies, axis, split_axis=0, concat_axis=0, tiled=True)  28.2 us
    psum x2, blocking collectives, over_axes(): return functools.reduce(lax.psum, axes, array)  17.2 us
    all_to_all x5, waiting for transfers between devices, copy_for_each(): return lax.all_to_all(copies, axis, split_axis=0, concat_axis=0, tiled=True)  15.2 us
    unnamed x70, local copies, waits for them, and re-layouts  10.6 us
    all_to_all x1, starting transfers between devices, sum_at_owner(): lax.all_to_all(blocks, axis, split_axis=0, concat_axis=0, tiled=True)  8.42 us
    dot_general x24, matrix products, extend(): jnp.einsum('bji,bik->bjk', parent_links, reached)  4.94 us
    convert_element_type x3, other arithmetic, combine_blocks(): merged = merged.reshape(values_first.shape).astype(jnp.bfloat16)  4.84 us
  transfers between devices with their start and end apart: 6, of which 4 were waited for; matrix products, arithmetic and copies ran while one was open for 40% of the time, Pallas kernels for 0%

commit v1 on v0

v1 whole, which is shorter than its diff:
```python
import functools

import jax
import jax.numpy as jnp
from jax import lax
from jax.experimental import pallas as pl
from jax.experimental.pallas import tpu as pltpu
from jax.sharding import PartitionSpec as P

D = 4096
HEAD = 64
QK = 32
SEQS = 4
PROP = 24
PAIRS = 4
LANES = 128
N_KV = 16
N_TP = 8
WINDOW = 48

f32 = jnp.float32
bf16 = jnp.bfloat16
epsilon = 1e-05
masked_low = -1e30
score_scale = QK ** (-0.5)
LOG2E = 1.4426950408889634

NT = (((1,), (1,)), ((), ()))
NN = (((1,), (0,)), ((), ()))


def iota(shape, dim):
    return lax.broadcasted_iota(jnp.int32, shape, dim)


def three_parts(row):
    wide = jnp.broadcast_to(row, (8, LANES))
    high = wide.astype(bf16).astype(f32)
    rest = wide - high
    middle = rest.astype(bf16).astype(f32)
    low = rest - middle
    place = iota((8, LANES), 0)
    tile = jnp.where(place == 0, high, jnp.where(place == 1, middle, jnp.where(place == 2, low, 0.0)))
    return tile.astype(bf16)


def column_to_row(column):
    count = column.shape[0]
    eye = iota((count, LANES), 0) == iota((count, LANES), 1)
    return jnp.sum(jnp.where(eye, column, 0.0), axis=0, keepdims=True)


def row_to_column(row, count):
    eye = iota((count, LANES), 0) == iota((count, LANES), 1)
    return jnp.sum(jnp.where(eye, row, 0.0), axis=1, keepdims=True)


def project_kernel(tokens, gain, w_query, w_key, w_value, out):
    wide = tokens[...].astype(f32)
    gained = (wide * gain[...]).astype(bf16)
    squares = jnp.sum(wide * wide, axis=1, keepdims=True)
    for place, weight in enumerate((w_query, w_key, w_value)):
        product = lax.dot_general(gained, weight[...], NN, preferred_element_type=f32).astype(bf16)
        for seq in range(SEQS):
            for pair in range(PAIRS):
                out[seq * PAIRS + pair, place * PROP : (place + 1) * PROP, :] = product[
                    seq * PROP : (seq + 1) * PROP, pair * LANES : (pair + 1) * LANES
                ]
    for seq in range(SEQS):
        tile = three_parts(column_to_row(squares[seq * PROP : (seq + 1) * PROP]))
        for pair in range(PAIRS):
            out[seq * PAIRS + pair, 3 * PROP :, :] = tile


def normalize_kernel(arrived, own, copies):
    total = arrived[0].astype(f32)
    for source in range(1, N_KV):
        total = total + arrived[source].astype(f32)
    row = total[72:73] + total[73:74] + total[74:75]
    factor = lax.rsqrt(row_to_column(row, PROP) / D + epsilon)
    for place in range(3):
        rows = slice(place * PROP, (place + 1) * PROP)
        part = (total[rows] * factor).astype(bf16)
        own[rows, :] = part
        for target in range(N_KV):
            copies[target, rows, :] = part


def expanded(queries, count):
    group = iota(queries.shape, 1) // QK
    zero = jnp.zeros_like(queries)
    return jnp.concatenate([jnp.where(group == place, queries, zero) for place in range(count)], axis=0)


def self_kernel(parents, own, out):
    pair_seq = lax.axis_index("kv") // PAIRS
    links = parents[pl.ds(pair_seq, 1), :].astype(f32)
    eye = (iota((PROP, PROP), 0) == iota((PROP, PROP), 1))
    column = jnp.sum(jnp.where(eye, jnp.broadcast_to(links, (PROP, PROP)), 0.0), axis=1, keepdims=True)
    reached = jnp.where(eye | (column == iota((PROP, PROP), 1).astype(f32)), 1.0, 0.0)
    for _ in range(5):
        narrow = reached.astype(bf16)
        reached = jnp.minimum(1.0, lax.dot_general(narrow, narrow, NN, preferred_element_type=f32))
    lineage = jnp.concatenate([reached] * 4, axis=0) > 0.5
    queries, keys, values = own[:PROP, :], own[PROP : 2 * PROP, :], own[2 * PROP :, :]
    scores = lax.dot_general(expanded(queries, 4), keys, NT, preferred_element_type=f32)
    scores = jnp.where(lineage, scores * score_scale, masked_low)
    largest = jnp.max(scores, axis=1, keepdims=True)
    weight = jnp.where(lineage, jnp.exp(scores - largest), 0.0)
    total = jnp.sum(weight, axis=1, keepdims=True)
    product = lax.dot_general(weight.astype(bf16), values, NN, preferred_element_type=f32) / total
    out[:48, :] = jnp.where(iota((48, LANES), 1) < HEAD, product[:48], product[48:])
    out[48:56, :] = jnp.broadcast_to(column_to_row(largest + jnp.log(total)), (8, LANES))


def attend_kernel(lengths, accepted, gathered, keys, values, out):
    seq, half = pl.program_id(0), pl.program_id(1)
    block_len = keys.shape[1]
    seen = lengths[seq] + accepted[seq] - lax.axis_index("kv") * block_len
    base = seq * PAIRS + half * 2
    queries = jnp.concatenate([gathered[base, :PROP, :], gathered[base + 1, :PROP, :]], axis=1)
    scores = lax.dot_general(expanded(queries, 8), keys[0], NT, preferred_element_type=f32)
    visible = iota((1, block_len), 1) < seen
    scores = jnp.where(visible, scores, masked_low)
    largest = jnp.max(scores, axis=1, keepdims=True)
    weight = jnp.exp2((scores - largest) * (score_scale * LOG2E))
    total = jnp.sum(weight, axis=1, keepdims=True)
    product = lax.dot_general(weight.astype(bf16), values[0], NN, preferred_element_type=f32) / total
    lane_head = iota((48, 2 * LANES), 1) // HEAD
    merged = jnp.where(lane_head == 0, product[:48], 0.0)
    for head in range(1, 4):
        merged = jnp.where(lane_head == head, product[head * 48 : (head + 1) * 48], merged)
    merged = merged.astype(bf16)
    level = jnp.where(seen > 0, largest * score_scale + jnp.log(total), masked_low)
    for pair in range(2):
        out[pair, :48, :] = merged[:, pair * LANES : (pair + 1) * LANES]
        out[pair, 48:, :] = three_parts(column_to_row(level[pair * 96 : (pair + 1) * 96]))


def finish_kernel(map_lambda, out_gain, arrived, own_part, copies):
    pair = lax.axis_index("kv") % PAIRS
    rows = []
    for source in range(N_KV):
        tile = arrived[source, 48:, :].astype(f32)
        rows.append(tile[0:1] + tile[1:2] + tile[2:3])
    rows.append(own_part[48:49, :])
    levels = jnp.concatenate(rows + [jnp.full((7, LANES), masked_low, f32)], axis=0)
    weights = jnp.exp(levels - jnp.max(levels, axis=0, keepdims=True))
    weights = weights / jnp.sum(weights, axis=0, keepdims=True)
    columns = jnp.concatenate([weights, jnp.zeros((LANES - 24, LANES), f32)], axis=0).T
    first = iota((48, LANES), 1) < HEAD
    total = jnp.zeros((48, LANES), f32)
    for source in range(N_KV + 1):
        factor = jnp.where(first, columns[:48, source : source + 1], columns[48:96, source : source + 1])
        part = arrived[source, :48, :].astype(f32) if source < N_KV else own_part[:48, :]
        total = total + factor * part
    lane_first = iota((PROP, LANES), 1) < HEAD
    lam = jnp.where(lane_first, map_lambda[2 * pair], map_lambda[2 * pair + 1])
    difference = total[:PROP] - lam * total[PROP:]
    squared = difference * difference
    mean_first = jnp.sum(jnp.where(lane_first, squared, 0.0), axis=1, keepdims=True)
    mean_second = jnp.sum(jnp.where(lane_first, 0.0, squared), axis=1, keepdims=True)
    mean = jnp.where(lane_first, mean_first, mean_second) / HEAD
    normed = (difference * lax.rsqrt(mean + epsilon) * out_gain[pl.ds(pair, 1), :]).astype(bf16)
    for target in range(N_KV):
        copies[target] = normed


def output_kernel(arrived, w_output, copies):
    total = None
    for pair in range(PAIRS):
        rows = jnp.concatenate([arrived[seq * PAIRS + pair] for seq in range(SEQS)], axis=0)
        part = lax.dot_general(
            rows, w_output[pair * LANES : (pair + 1) * LANES, :], NN, preferred_element_type=f32
        )
        total = part if total is None else total + part
    total = total.astype(bf16)
    for target in range(N_TP):
        copies[target] = total


def mix_kernel(arrived, out):
    total = arrived[0].astype(f32)
    for source in range(1, N_TP):
        total = total + arrived[source].astype(f32)
    out[...] = total.astype(bf16)


def write_kernel(lengths, accepted, gathered, keys, values, new_keys, new_values):
    seq = pl.program_id(0)
    block_len = keys.shape[1]
    begin = lengths[seq] + accepted[seq] - lax.axis_index("kv") * block_len
    new_keys[...] = keys[...]
    new_values[...] = values[...]

    @pl.when((begin > -PROP) & (begin < block_len))
    def _():
        base = pl.multiple_of(jnp.clip((begin // 16) * 16, 0, block_len - WINDOW), 16)
        slot = base - begin + iota((WINDOW, PROP), 0)
        placing = (slot == iota((WINDOW, PROP), 1)).astype(bf16)
        row = base - begin + iota((WINDOW, LANES), 0)
        written = (row >= 0) & (row < PROP)
        for place, target in ((1, new_keys), (2, new_values)):
            for pair in range(PAIRS):
                lanes = slice(pair * LANES, (pair + 1) * LANES)
                rows = gathered[seq * PAIRS + pair, place * PROP : (place + 1) * PROP, :]
                moved = lax.dot_general(placing, rows, NN, preferred_element_type=f32)
                old = target[0, pl.ds(base, WINDOW), lanes]
                target[0, pl.ds(base, WINDOW), lanes] = jnp.where(written, moved, old.astype(f32)).astype(bf16)


def vmem():
    return pl.BlockSpec(memory_space=pltpu.VMEM)


def smem():
    return pl.BlockSpec(memory_space=pltpu.SMEM)


def shape(dims, kind=bf16):
    return jax.ShapeDtypeStruct(dims, kind)


def room(mebibytes):
    return pltpu.CompilerParams(vmem_limit_bytes=mebibytes * 1024 * 1024)


def cost(flops, moved):
    return pl.CostEstimate(flops=flops, bytes_accessed=moved, transcendentals=0)


def local(
    tokens,
    norm_gain,
    w_query,
    w_key,
    w_value,
    w_output,
    cache_keys,
    cache_values,
    map_lambda,
    out_gain,
    parents,
    lengths,
    accepted,
):
    block_len = cache_keys.shape[1]
    width = cache_keys.shape[2]
    exchange = functools.partial(lax.all_to_all, split_axis=0, concat_axis=0, tiled=True)

    partial = pl.pallas_call(
        project_kernel,
        out_shape=shape((N_KV, 80, LANES)),
        in_specs=[vmem()] * 5,
        out_specs=vmem(),
        compiler_params=room(8),
        name="project",
    )(tokens, norm_gain.reshape(1, -1), w_query, w_key, w_value)
    arrived = exchange(partial, "kv")
    own, copies = pl.pallas_call(
        normalize_kernel,
        out_shape=(shape((72, LANES)), shape((N_KV, 72, LANES))),
        in_specs=[vmem()],
        out_specs=(vmem(), vmem()),
        compiler_params=room(8),
        name="normalize",
    )(arrived)
    gathered = exchange(copies, "kv")
    own_part = pl.pallas_call(
        self_kernel,
        out_shape=shape((56, LANES), f32),
        in_specs=[vmem(), vmem()],
        out_specs=vmem(),
        cost_estimate=cost(4_000_000_000, 100_000),
        compiler_params=room(8),
        name="own_scores",
    )(parents, own)
    cache_block = pl.BlockSpec((1, block_len, 2 * LANES), lambda seq, half: (seq, 0, half))
    parts = pl.pallas_call(
        attend_kernel,
        grid=(SEQS, 2),
        out_shape=shape((N_KV, 56, LANES)),
        in_specs=[smem(), smem(), vmem(), cache_block, cache_block],
        out_specs=pl.BlockSpec((2, 56, LANES), lambda seq, half: (seq * 2 + half, 0, 0)),
        compiler_params=room(16),
        name="attend",
    )(lengths, accepted, gathered, cache_keys, cache_values)
    arrived_parts = exchange(parts, "kv")
    whole = pl.BlockSpec((1, block_len, width), lambda seq: (seq, 0, 0))
    new_keys, new_values = pl.pallas_call(
        write_kernel,
        grid=(SEQS,),
        out_shape=(shape(cache_keys.shape), shape(cache_values.shape)),
        in_specs=[smem(), smem(), vmem(), whole, whole],
        out_specs=(whole, whole),
        cost_estimate=cost(8_000_000_000, 8_000_000),
        compiler_params=room(16),
        name="write",
    )(lengths, accepted, gathered, cache_keys, cache_values)
    normed = pl.pallas_call(
        finish_kernel,
        out_shape=shape((N_KV, PROP, LANES)),
        in_specs=[smem(), vmem(), vmem(), vmem()],
        out_specs=vmem(),
        compiler_params=room(8),
        name="finish",
    )(map_lambda, out_gain.reshape(PAIRS, LANES), arrived_parts, own_part)
    arrived_normed = exchange(normed, "kv")
    partial_out = pl.pallas_call(
        output_kernel,
        out_shape=shape((N_TP, SEQS * PROP, w_output.shape[1])),
        in_specs=[vmem(), vmem()],
        out_specs=vmem(),
        compiler_params=room(8),
        name="output",
    )(arrived_normed, w_output)
    arrived_out = exchange(partial_out, "tp")
    mixed = pl.pallas_call(
        mix_kernel,
        out_shape=shape((SEQS * PROP, w_output.shape[1])),
        in_specs=[vmem()],
        out_specs=vmem(),
        compiler_params=room(8),
        name="mix",
    )(arrived_out)
    return (mixed, new_keys, new_values)


def solution(mesh):
    return jax.shard_map(
        local,
        mesh=mesh,
        in_specs=(
            P(None, "kv"),
            P("kv"),
            P("kv", "tp"),
            P("kv", "tp"),
            P("kv", "tp"),
            P("tp", "kv"),
            P(None, "kv", "tp"),
            P(None, "kv", "tp"),
            P("tp"),
            P("tp"),
            P(),
            P(),
            P(),
        ),
        out_specs=(P(None, "kv"), P(None, "kv", "tp"), P(None, "kv", "tp")),
        check_vma=False,
    )
```

time: 162 us -> 81.3 us (0.50)
  local copies, waits for them, and re-layouts: 60 us -> 7.68 us
  starting transfers between devices: 36.6 us -> 13.4 us
  blocking collectives: 17.2 us -> 36.7 us
  matrix products: 18.4 us -> 0 us
  Pallas kernels: 0 us -> 12.6 us
  other arithmetic: 11.5 us -> 0 us
  waiting for transfers between devices: 15.2 us -> 9.5 us
    mul x22 -> x0, local copies, waits for them, and re-layouts: 37.9 us -> none  [the longest x18 37.5 us: scaled_values(): return shaped * jnp.transpose(factor, (0, 1, 3, 2))[..., None]]
    all_to_all x0 -> x3, blocking collectives: none -> 36.7 us  [the longest x1 16.7 us: local(): arrived = exchange(partial, 'kv')]
    all_to_all x6 -> x2, starting transfers between devices: 36.6 us -> 13.4 us  [the longest x1 9.92 us: local(): arrived_out = exchange(partial_out, 'tp')]
    dot_general x34 -> x0, matrix products: 18.4 us -> none  [the longest x24 4.94 us: extend(): jnp.einsum('bji,bik->bjk', parent_links, reached)]
    psum x2 -> x0, blocking collectives: 17.2 us -> none  [over_axes(): return functools.reduce(lax.psum, axes, array)]
    pallas_call x0 -> x8, Pallas kernels: none -> 12.6 us  [the longest x1 5.56 us: local(): pl.pallas_call(attend_kernel, grid=(SEQS, 2), out_shape=shape((N_KV, 56,...]
    all_to_all x6 -> x2, waiting for transfers between devices: 15.2 us -> 9.5 us  [the longest x1 6.36 us: local(): arrived_parts = exchange(parts, 'kv')]
    convert_element_type x8 -> x0, other arithmetic: 5.11 us -> none  [the longest x3 4.84 us: combine_blocks(): merged = merged.reshape(values_first.shape).astype(jnp.bfloat16)]
  transfers between devices with their start and end apart: 6 -> 2, of which waited for: 4 -> 2; matrix products, arithmetic and copies ran while one was open for 40% -> 0% of each run, Pallas kernels for 0% -> 5%
where the time goes in v1:
time: 81.3 us; the launch traced here: 80.7 us
  blocking collectives  36.7 us (45%)
  starting transfers between devices  13.4 us (16%)
  Pallas kernels  12.6 us (15%)
  waiting for transfers between devices  9.5 us (12%)
  local copies, waits for them, and re-layouts  7.68 us (9%)
    all_to_all x1, blocking collectives, local(): arrived = exchange(partial, 'kv')  16.7 us
    all_to_all x1, blocking collectives, local(): gathered = exchange(copies, 'kv')  10.7 us
    all_to_all x1, starting transfers between devices, local(): arrived_out = exchange(partial_out, 'tp')  9.92 us
    all_to_all x1, blocking collectives, local(): arrived_normed = exchange(normed, 'kv')  9.33 us
    unnamed x28, local copies, waits for them, and re-layouts  7.68 us
    all_to_all x1, waiting for transfers between devices, local(): arrived_parts = exchange(parts, 'kv')  6.36 us
    pallas_call x1, Pallas kernels, local(): pl.pallas_call(attend_kernel, grid=(SEQS, 2), out_shape=shape((N_KV, 56,...  5.56 us
    all_to_all x1, starting transfers between devices, local(): arrived_parts = exchange(parts, 'kv')  3.53 us
  transfers between devices with their start and end apart: 2, of which 2 were waited for; matrix products, arithmetic and copies ran while one was open for 0% of the time, Pallas kernels for 5%

profile of v1, /device:TPU:1, one launch (start us, length us, event | category | flops | bytes accessed | tf_op | source)
XLA Modules:
  0.0 80.7 jit_solution(11687978668200982773)
XLA Ops:
  0.7 1.1 %copy-done.4 = bf16[256,512]{1,0:T(8,128)(2,1)S(1)} copy-done((bf16[256,512]{1,0:T(8,128)(2,1)S(1)}, bf16[256,512]{1,0:T(8,128)(2,1)}, u32[]{:S(2)}) %copy-start.4) | copy-done | bytes 262168
  1.7 0.9 %copy-done.5 = bf16[256,512]{1,0:T(8,128)(2,1)S(1)} copy-done((bf16[256,512]{1,0:T(8,128)(2,1)S(1)}, bf16[256,512]{1,0:T(8,128)(2,1)}, u32[]{:S(2)}) %copy-start.5) | copy-done | bytes 262168
  2.7 0.9 %copy-done.6 = bf16[256,512]{1,0:T(8,128)(2,1)S(1)} copy-done((bf16[256,512]{1,0:T(8,128)(2,1)S(1)}, bf16[256,512]{1,0:T(8,128)(2,1)}, u32[]{:S(2)}) %copy-start.6) | copy-done | bytes 262168
  3.6 0.8 copy-done.7
  4.4 0.7 copy-done.9
  5.1 0.3 project.1
  5.4 16.7 %all_to_all.25.arrived = bf16[16,80,128]{2,1,0:T(8,128)(2,1)S(1)} all-to-all(bf16[16,80,128]{2,1,0:T(8,128)(2,1)S(1)} %project.1), channel_id=1, replica_groups=mesh['kv'=16,'tp'=8] {'kv'}, dimensions={0} | all-to-all | bytes 655360 | tf_op jit(solution)/shard_map/all_to_all | solution.py:259
  22.1 0.1 normalize.1
  22.3 10.7 %all_to_all.26.gathered = bf16[16,72,128]{2,1,0:T(8,128)(2,1)S(1)} all-to-all(bf16[16,72,128]{2,1,0:T(8,128)(2,1)S(1)} %get-tuple-element.7), channel_id=1, replica_groups=mesh['kv'=16,'tp'=8] {'kv'}, dimensions={0} | all-to-all | bytes 589824 | tf_op jit(solution)/shard_map/all_to_all | solution.py:268
  32.9 0.0 copy-start.1
  33.0 1.6 %copy-done.1 = bf16[4,512,512]{2,1,0:T(8,128)(2,1)S(1)} copy-done((bf16[4,512,512]{2,1,0:T(8,128)(2,1)S(1)}, bf16[4,512,512]{2,1,0:T(8,128)(2,1)}, u32[]{:S(2)}) %copy-start.1) | copy-done | bytes 2097176
  34.5 5.6 %attend.1 = bf16[16,56,128]{2,1,0:T(8,128)(2,1)} custom-call(s32[4]{0:T(128)S(1)} %copy-done.11, s32[4]{0:T(128)S(1)} %copy-done.12, bf16[16,72,128]{2,1,0:T(8,128)(2,1)S(1)} %all_to_all.26.gathered, bf16[4,512,512]{2,1,0:T(8,128)(2,1)S(1)} %copy-done, bf16[4,512,512]{2,1,0:T(8,128)(2,1)S(1)} %copy-done.1), custom_call_target="tpu_custom_call" | custom-call | tf_op jit(solution)/shard_map/attend/pallas_call | solution.py:279
  40.1 3.5 %all-to-all-start.2 = ((bf16[16,56,128]{2,1,0:T(8,128)(2,1)}), bf16[16,56,128]{2,1,0:T(8,128)(2,1)S(1)}, u32[]{:S(2)}, u32[]{:S(2)}) async-start(bf16[16,56,128]{2,1,0:T(8,128)(2,1)} %attend.1), calls=%async_computation.2 | async-start | bytes 458752 | tf_op jit(solution)/shard_map/all_to_all | solution.py:288
  43.6 0.0 copy-start.8
  43.7 0.9 %own_scores.1.own_part = f32[56,128]{1,0:T(8,128)S(1)} custom-call(s32[4,24]{1,0:T(4,128)S(1)} %copy-done.13, bf16[72,128]{1,0:T(8,128)(2,1)S(1)} %get-tuple-element.8.own), custom_call_target="tpu_custom_call" | custom-call | flops 4000000000 | bytes 100000 | tf_op jit(solution)/shard_map/own_scores/pallas_call | solution.py:269
  44.6 6.4 %all-to-all-done.2.arrived = bf16[16,56,128]{2,1,0:T(8,128)(2,1)S(1)} async-done(((bf16[16,56,128]{2,1,0:T(8,128)(2,1)}), bf16[16,56,128]{2,1,0:T(8,128)(2,1)S(1)}, u32[]{:S(2)}, u32[]{:S(2)}) %all-to-all-start.2) | async-done | bytes 229408 | tf_op jit(solution)/shard_map/all_to_all | solution.py:288
  51.0 1.1 %finish.1 = bf16[16,24,128]{2,1,0:T(8,128)(2,1)S(1)} custom-call(f32[8]{0:T(128)S(1)} %copy-done.10, f32[4,128]{1,0:T(4,128)S(1)} %bitcast.2, bf16[16,56,128]{2,1,0:T(8,128)(2,1)S(1)} %all-to-all-done.2.arrived, f32[56,128]{1,0:T(8,128)S(1)} %own_scores.1.own_part), custom_call_target="tpu_custom_call" | custom-call | tf_op jit(solution)/shard_map/finish/pallas_call | solution.py:300
  52.1 9.3 %all_to_all.27.arrived = bf16[16,24,128]{2,1,0:T(8,128)(2,1)S(1)} all-to-all(bf16[16,24,128]{2,1,0:T(8,128)(2,1)S(1)} %finish.1), channel_id=1, replica_groups=mesh['kv'=16,'tp'=8] {'kv'}, dimensions={0} | all-to-all | bytes 196608 | tf_op jit(solution)/shard_map/all_to_all | solution.py:308
  61.4 0.9 %output.1 = bf16[8,96,256]{2,1,0:T(8,128)(2,1)} custom-call(bf16[16,24,128]{2,1,0:T(8,128)(2,1)S(1)} %all_to_all.27.arrived, bf16[512,256]{1,0:T(8,128)(2,1)S(1)} %copy-done.3), custom_call_target="tpu_custom_call" | custom-call | tf_op jit(solution)/shard_map/output/pallas_call | solution.py:309
  62.4 9.9 %all-to-all-start.4 = ((bf16[8,96,256]{2,1,0:T(8,128)(2,1)}), bf16[8,96,256]{2,1,0:T(8,128)(2,1)S(1)}, u32[]{:S(2)}, u32[]{:S(2)}) async-start(bf16[8,96,256]{2,1,0:T(8,128)(2,1)} %output.1), calls=%async_computation.4 | async-start | bytes 786432 | tf_op jit(solution)/shard_map/all_to_all | solution.py:317
  72.3 1.6 %copy-done.2 = bf16[4,512,512]{2,1,0:T(8,128)(2,1)S(1)} copy-done((bf16[4,512,512]{2,1,0:T(8,128)(2,1)S(1)}, bf16[4,512,512]{2,1,0:T(8,128)(2,1)}, u32[]{:S(2)}) %copy-start.2) | copy-done | bytes 2097176
  73.9 3.0 %write.1 = (bf16[4,512,512]{2,1,0:T(8,128)(2,1)}, bf16[4,512,512]{2,1,0:T(8,128)(2,1)}) custom-call(s32[4]{0:T(128)S(1)} %copy-done.11, s32[4]{0:T(128)S(1)} %copy-done.12, bf16[16,72,128]{2,1,0:T(8,128)(2,1)S(1)} %all_to_all.26.gathered, bf16[4,512,512]{2,1,0:T(8,128)(2,1)S(1)} %copy-done, bf16[4,512,512]{2,1,0:T(8,128)(2,1)S(1)} %copy-done.2), custom_call_target="tpu_custom_call" | custom-call | flops 8000000000 | bytes 8000000 | tf_op jit(solution)/shard_map/write/pallas_call | solution.py:290
  76.8 3.1 %all-to-all-done.4.arrived = bf16[8,96,256]{2,1,0:T(8,128)(2,1)S(1)} async-done(((bf16[8,96,256]{2,1,0:T(8,128)(2,1)}), bf16[8,96,256]{2,1,0:T(8,128)(2,1)S(1)}, u32[]{:S(2)}, u32[]{:S(2)}) %all-to-all-start.4) | async-done | bytes 393248 | tf_op jit(solution)/shard_map/all_to_all | solution.py:317
  80.0 0.7 mix.1
  (19 shorter events, 0.0 us)
Async XLA Ops:
  0.6 32.3 %copy-start = (bf16[4,512,512]{2,1,0:T(8,128)(2,1)S(1)}, bf16[4,512,512]{2,1,0:T(8,128)(2,1)}, u32[]{:S(2)}) copy-start(bf16[4,512,512]{2,1,0:T(8,128)(2,1)} %keys.3) | copy-start | bytes 6291460
  0.6 1.1 %copy-start.4 = (bf16[256,512]{1,0:T(8,128)(2,1)S(1)}, bf16[256,512]{1,0:T(8,128)(2,1)}, u32[]{:S(2)}) copy-start(bf16[256,512]{1,0:T(8,128)(2,1)} %w_query.1) | copy-start | bytes 786436
  1.7 0.9 %copy-start.5 = (bf16[256,512]{1,0:T(8,128)(2,1)S(1)}, bf16[256,512]{1,0:T(8,128)(2,1)}, u32[]{:S(2)}) copy-start(bf16[256,512]{1,0:T(8,128)(2,1)} %w_key.1) | copy-start | bytes 786436
  2.7 0.9 %copy-start.6 = (bf16[256,512]{1,0:T(8,128)(2,1)S(1)}, bf16[256,512]{1,0:T(8,128)(2,1)}, u32[]{:S(2)}) copy-start(bf16[256,512]{1,0:T(8,128)(2,1)} %w_value.1) | copy-start | bytes 786436
  3.6 0.8 copy-start.7
  4.4 0.7 copy-start.9
  5.1 27.8 %copy-start.11 = (s32[4]{0:T(128)S(1)}, s32[4]{0:T(128)}, u32[]{:S(2)}) copy-start(s32[4]{0:T(128)} %lengths.3) | copy-start | bytes 52
  5.1 27.8 %copy-start.12 = (s32[4]{0:T(128)S(1)}, s32[4]{0:T(128)}, u32[]{:S(2)}) copy-start(s32[4]{0:T(128)} %accepted.3) | copy-start | bytes 52
  32.9 1.6 %copy-start.1 = (bf16[4,512,512]{2,1,0:T(8,128)(2,1)S(1)}, bf16[4,512,512]{2,1,0:T(8,128)(2,1)}, u32[]{:S(2)}) copy-start(bf16[4,512,512]{2,1,0:T(8,128)(2,1)} %values.3) | copy-start | bytes 6291460
  34.5 9.1 %copy-start.13 = (s32[4,24]{1,0:T(4,128)S(1)}, s32[4,24]{1,0:T(4,128)}, u32[]{:S(2)}) copy-start(s32[4,24]{1,0:T(4,128)} %parents.1) | copy-start | bytes 1156
  40.1 10.9 %all-to-all-start.2 = ((bf16[16,56,128]{2,1,0:T(8,128)(2,1)}), bf16[16,56,128]{2,1,0:T(8,128)(2,1)S(1)}, u32[]{:S(2)}, u32[]{:S(2)}) async-start(bf16[16,56,128]{2,1,0:T(8,128)(2,1)} %attend.1), calls=%async_computation.2 | async-start | bytes 458752 | tf_op jit(solution)/shard_map/all_to_all | solution.py:288
  43.6 7.3 %copy-start.8 = (f32[512]{0:T(512)S(1)}, f32[512]{0:T(512)}, u32[]{:S(2)}) copy-start(f32[512]{0:T(512)} %param.22) | copy-start | bytes 6148
  43.7 7.3 %copy-start.10 = (f32[8]{0:T(128)S(1)}, f32[8]{0:T(128)}, u32[]{:S(2)}) copy-start(f32[8]{0:T(128)} %map_lambda.1) | copy-start | bytes 100
  43.7 17.7 %copy-start.3 = (bf16[512,256]{1,0:T(8,128)(2,1)S(1)}, bf16[512,256]{1,0:T(8,128)(2,1)}, u32[]{:S(2)}) copy-start(bf16[512,256]{1,0:T(8,128)(2,1)} %w_output.1) | copy-start | bytes 786436
  62.4 17.6 %all-to-all-start.4 = ((bf16[8,96,256]{2,1,0:T(8,128)(2,1)}), bf16[8,96,256]{2,1,0:T(8,128)(2,1)S(1)}, u32[]{:S(2)}, u32[]{:S(2)}) async-start(bf16[8,96,256]{2,1,0:T(8,128)(2,1)} %output.1), calls=%async_computation.4 | async-start | bytes 786432 | tf_op jit(solution)/shard_map/all_to_all | solution.py:317
  72.3 1.6 %copy-start.2 = (bf16[4,512,512]{2,1,0:T(8,128)(2,1)S(1)}, bf16[4,512,512]{2,1,0:T(8,128)(2,1)}, u32[]{:S(2)}) copy-start(bf16[4,512,512]{2,1,0:T(8,128)(2,1)} %values.3) | copy-start | bytes 6291460

commit v2 on v1

--- a/solution.py
+++ b/solution.py
@@ -55,11 +55,19 @@
     return jnp.sum(jnp.where(eye, row, 0.0), axis=1, keepdims=True)
 
 
-def project_kernel(tokens, gain, w_query, w_key, w_value, out):
+def project_kernel(tokens_far, gain_far, query_far, key_far, value_far, out, tokens, gain, query, key, value, done):
+    far = (tokens_far, gain_far, query_far, key_far, value_far)
+    near = (tokens, gain, query, key, value)
+    loads = [pltpu.make_async_copy(a, b, done.at[place]) for place, (a, b) in enumerate(zip(far, near))]
+    for load in loads:
+        load.start()
+    loads[0].wait()
+    loads[1].wait()
     wide = tokens[...].astype(f32)
     gained = (wide * gain[...]).astype(bf16)
     squares = jnp.sum(wide * wide, axis=1, keepdims=True)
-    for place, weight in enumerate((w_query, w_key, w_value)):
+    for place, weight in enumerate((query, key, value)):
+        loads[2 + place].wait()
         product = lax.dot_general(gained, weight[...], NN, preferred_element_type=f32).astype(bf16)
         for seq in range(SEQS):
             for pair in range(PAIRS):
@@ -92,7 +100,7 @@
     return jnp.concatenate([jnp.where(group == place, queries, zero) for place in range(count)], axis=0)
 
 
-def self_kernel(parents, own, out):
+def own_scores(parents, own, out):
     pair_seq = lax.axis_index("kv") // PAIRS
     links = parents[pl.ds(pair_seq, 1), :].astype(f32)
     eye = (iota((PROP, PROP), 0) == iota((PROP, PROP), 1))
@@ -113,28 +121,110 @@
     out[48:56, :] = jnp.broadcast_to(column_to_row(largest + jnp.log(total)), (8, LANES))
 
 
-def attend_kernel(lengths, accepted, gathered, keys, values, out):
-    seq, half = pl.program_id(0), pl.program_id(1)
+def attend_kernel(
+    lengths,
+    accepted,
+    gathered,
+    keys,
+    values_far,
+    parents,
+    own,
+    out,
+    new_keys,
+    new_values,
+    own_part,
+    values,
+    window,
+    loaded,
+    stored,
+    patched,
+):
     block_len = keys.shape[1]
-    seen = lengths[seq] + accepted[seq] - lax.axis_index("kv") * block_len
-    base = seq * PAIRS + half * 2
-    queries = jnp.concatenate([gathered[base, :PROP, :], gathered[base + 1, :PROP, :]], axis=1)
-    scores = lax.dot_general(expanded(queries, 8), keys[0], NT, preferred_element_type=f32)
-    visible = iota((1, block_len), 1) < seen
-    scores = jnp.where(visible, scores, masked_low)
-    largest = jnp.max(scores, axis=1, keepdims=True)
-    weight = jnp.exp2((scores - largest) * (score_scale * LOG2E))
-    total = jnp.sum(weight, axis=1, keepdims=True)
-    product = lax.dot_general(weight.astype(bf16), values[0], NN, preferred_element_type=f32) / total
+    offset = lax.axis_index("kv") * block_len
+    loads = [pltpu.make_async_copy(values_far.at[seq], values.at[seq], loaded.at[seq]) for seq in range(SEQS)]
+    stores = [
+        pltpu.make_async_copy(source.at[seq], target.at[seq], stored.at[seq, place])
+        for seq in range(SEQS)
+        for place, (source, target) in enumerate(((keys, new_keys), (values, new_values)))
+    ]
+    for load in loads:
+        load.start()
+    begins = [lengths[seq] + accepted[seq] - offset for seq in range(SEQS)]
+    bases = [pl.multiple_of(jnp.clip((begin // 16) * 16, 0, block_len - WINDOW), 16) for begin in begins]
+    here = [(begin > -PROP) & (begin < block_len) for begin in begins]
+
+    def patches(seq):
+        return [
+            pltpu.make_async_copy(
+                window.at[seq, place], target.at[seq, pl.ds(bases[seq], WINDOW)], patched.at[seq, place]
+            )
+            for place, target in enumerate((new_keys, new_values))
+        ]
+
     lane_head = iota((48, 2 * LANES), 1) // HEAD
-    merged = jnp.where(lane_head == 0, product[:48], 0.0)
-    for head in range(1, 4):
-        merged = jnp.where(lane_head == head, product[head * 48 : (head + 1) * 48], merged)
-    merged = merged.astype(bf16)
-    level = jnp.where(seen > 0, largest * score_scale + jnp.log(total), masked_low)
-    for pair in range(2):
-        out[pair, :48, :] = merged[:, pair * LANES : (pair + 1) * LANES]
-        out[pair, 48:, :] = three_parts(column_to_row(level[pair * 96 : (pair + 1) * 96]))
+    for seq in range(SEQS):
+        stores[2 * seq].start()
+        visible = iota((1, block_len), 1) < begins[seq]
+        weights = []
+        for half in range(2):
+            base = seq * PAIRS + half * 2
+            lanes = slice(half * 2 * LANES, (half + 1) * 2 * LANES)
+            queries = jnp.concatenate([gathered[base, :PROP, :], gathered[base + 1, :PROP, :]], axis=1)
+            scores = lax.dot_general(expanded(queries, 8), keys[seq, :, lanes], NT, preferred_element_type=f32)
+            scores = jnp.where(visible, scores, masked_low)
+            largest = jnp.max(scores, axis=1, keepdims=True)
+            weight = jnp.exp2((scores - largest) * (score_scale * LOG2E))
+            total = jnp.sum(weight, axis=1, keepdims=True)
+            level = jnp.where(begins[seq] > 0, largest * score_scale + jnp.log(total), masked_low)
+            for pair in range(2):
+                out[base + pair, 48:, :] = three_parts(column_to_row(level[pair * 96 : (pair + 1) * 96]))
+            weights.append((weight.astype(bf16), 1.0 / total))
+        loads[seq].wait()
+        stores[2 * seq + 1].start()
+        for half in range(2):
+            base = seq * PAIRS + half * 2
+            lanes = slice(half * 2 * LANES, (half + 1) * 2 * LANES)
+            weight, inverse = weights[half]
+            product = lax.dot_general(weight, values[seq, :, lanes], NN, preferred_element_type=f32)
+            merged = jnp.where(lane_head == 0, product[:48] * inverse[:48], 0.0)
+            for head in range(1, 4):
+                rows = slice(head * 48, (head + 1) * 48)
+                merged = jnp.where(lane_head == head, product[rows] * inverse[rows], merged)
+            merged = merged.astype(bf16)
+            for pair in range(2):
+                out[base + pair, :48, :] = merged[:, pair * LANES : (pair + 1) * LANES]
+    for seq in range(SEQS):
+
+        @pl.when(here[seq])
+        def _():
+            shift = bases[seq] - begins[seq]
+            placing = (shift + iota((WINDOW, PROP), 0) == iota((WINDOW, PROP), 1)).astype(bf16)
+            row = shift + iota((WINDOW, LANES), 0)
+            written = (row >= 0) & (row < PROP)
+            for place, source in ((0, keys), (1, values)):
+                for pair in range(PAIRS):
+                    lanes = slice(pair * LANES, (pair + 1) * LANES)
+                    rows = gathered[seq * PAIRS + pair, (place + 1) * PROP : (place + 2) * PROP, :]
+                    moved = lax.dot_general(placing, rows, NN, preferred_element_type=f32)
+                    old = source[seq, pl.ds(bases[seq], WINDOW), lanes].astype(f32)
+                    window[seq, place, :, lanes] = jnp.where(written, moved, old).astype(bf16)
+
+    for store in stores:
+        store.wait()
+    for seq in range(SEQS):
+
+        @pl.when(here[seq])
+        def _():
+            for patch in patches(seq):
+                patch.start()
+
+    own_scores(parents, own, own_part)
+    for seq in range(SEQS):
+
+        @pl.when(here[seq])
+        def _():
+            for patch in patches(seq):
+                patch.wait()
 
 
 def finish_kernel(map_lambda, out_gain, arrived, own_part, copies):
@@ -186,33 +276,14 @@
     out[...] = total.astype(bf16)
 
 
-def write_kernel(lengths, accepted, gathered, keys, values, new_keys, new_values):
-    seq = pl.program_id(0)
-    block_len = keys.shape[1]
-    begin = lengths[seq] + accepted[seq] - lax.axis_index("kv") * block_len
-    new_keys[...] = keys[...]
-    new_values[...] = values[...]
-
-    @pl.when((begin > -PROP) & (begin < block_len))
-    def _():
-        base = pl.multiple_of(jnp.clip((begin // 16) * 16, 0, block_len - WINDOW), 16)
-        slot = base - begin + iota((WINDOW, PROP), 0)
-        placing = (slot == iota((WINDOW, PROP), 1)).astype(bf16)
-        row = base - begin + iota((WINDOW, LANES), 0)
-        written = (row >= 0) & (row < PROP)
-        for place, target in ((1, new_keys), (2, new_values)):
-            for pair in range(PAIRS):
-                lanes = slice(pair * LANES, (pair + 1) * LANES)
-                rows = gathered[seq * PAIRS + pair, place * PROP : (place + 1) * PROP, :]
-                moved = lax.dot_general(placing, rows, NN, preferred_element_type=f32)
-                old = target[0, pl.ds(base, WINDOW), lanes]
-                target[0, pl.ds(base, WINDOW), lanes] = jnp.where(written, moved, old.astype(f32)).astype(bf16)
-
-
 def vmem():
     return pl.BlockSpec(memory_space=pltpu.VMEM)
 
 
+def hbm():
+    return pl.BlockSpec(memory_space=pltpu.HBM)
+
+
 def smem():
     return pl.BlockSpec(memory_space=pltpu.SMEM)
 
@@ -223,6 +294,14 @@
 
 def room(mebibytes):
     return pltpu.CompilerParams(vmem_limit_bytes=mebibytes * 1024 * 1024)
+
+
+def near(dims, kind=bf16):
+    return pltpu.VMEM(dims, kind)
+
+
+def far(*arrays):
+    return [pltpu.with_memory_space_constraint(array, pltpu.HBM) for array in arrays]
 
 
 def cost(flops, moved):
@@ -244,62 +323,60 @@
     lengths,
     accepted,
 ):
-    block_len = cache_keys.shape[1]
     width = cache_keys.shape[2]
     exchange = functools.partial(lax.all_to_all, split_axis=0, concat_axis=0, tiled=True)
 
     partial = pl.pallas_call(
         project_kernel,
-        out_shape=shape((N_KV, 80, LANES)),
-        in_specs=[vmem()] * 5,
+        out_shape=near((N_KV, 80, LANES)),
+        in_specs=[hbm()] * 5,
         out_specs=vmem(),
+        scratch_shapes=[
+            pltpu.VMEM(tokens.shape, bf16),
+            pltpu.VMEM((1, norm_gain.shape[0]), f32),
+            pltpu.VMEM(w_query.shape, bf16),
+            pltpu.VMEM(w_key.shape, bf16),
+            pltpu.VMEM(w_value.shape, bf16),
+            pltpu.SemaphoreType.DMA((5,)),
+        ],
         compiler_params=room(8),
         name="project",
-    )(tokens, norm_gain.reshape(1, -1), w_query, w_key, w_value)
+    )(*far(tokens, norm_gain.reshape(1, -1), w_query, w_key, w_value))
+    near_keys = pltpu.with_memory_space_constraint(cache_keys, pltpu.VMEM)
     arrived = exchange(partial, "kv")
     own, copies = pl.pallas_call(
         normalize_kernel,
-        out_shape=(shape((72, LANES)), shape((N_KV, 72, LANES))),
+        out_shape=(near((72, LANES)), near((N_KV, 72, LANES))),
         in_specs=[vmem()],
         out_specs=(vmem(), vmem()),
         compiler_params=room(8),
         name="normalize",
     )(arrived)
     gathered = exchange(copies, "kv")
-    own_part = pl.pallas_call(
-        self_kernel,
-        out_shape=shape((56, LANES), f32),
-        in_specs=[vmem(), vmem()],
-        out_specs=vmem(),
-        cost_estimate=cost(4_000_000_000, 100_000),
-        compiler_params=room(8),
-        name="own_scores",
-    )(parents, own)
-    cache_block = pl.BlockSpec((1, block_len, 2 * LANES), lambda seq, half: (seq, 0, half))
-    parts = pl.pallas_call(
+    parts, new_keys, new_values, own_part = pl.pallas_call(
         attend_kernel,
-        grid=(SEQS, 2),
-        out_shape=shape((N_KV, 56, LANES)),
-        in_specs=[smem(), smem(), vmem(), cache_block, cache_block],
-        out_specs=pl.BlockSpec((2, 56, LANES), lambda seq, half: (seq * 2 + half, 0, 0)),
-        compiler_params=room(16),
+        out_shape=(
+            near((N_KV, 56, LANES)),
+            shape(cache_keys.shape),
+            shape(cache_values.shape),
+            near((56, LANES), f32),
+        ),
+        in_specs=[smem(), smem(), vmem(), vmem(), hbm(), vmem(), vmem()],
+        out_specs=(vmem(), hbm(), hbm(), vmem()),
+        scratch_shapes=[
+            pltpu.VMEM(cache_values.shape, bf16),
+            pltpu.VMEM((SEQS, 2, WINDOW, width), bf16),
+            pltpu.SemaphoreType.DMA((SEQS,)),
+            pltpu.SemaphoreType.DMA((SEQS, 2)),
+            pltpu.SemaphoreType.DMA((SEQS, 2)),
+        ],
+        compiler_params=room(24),
         name="attend",
-    )(lengths, accepted, gathered, cache_keys, cache_values)
+    )(lengths, accepted, gathered, near_keys, *far(cache_values), parents, own)
     arrived_parts = exchange(parts, "kv")
-    whole = pl.BlockSpec((1, block_len, width), lambda seq: (seq, 0, 0))
-    new_keys, new_values = pl.pallas_call(
-        write_kernel,
-        grid=(SEQS,),
-        out_shape=(shape(cache_keys.shape), shape(cache_values.shape)),
-        in_specs=[smem(), smem(), vmem(), whole, whole],
-        out_specs=(whole, whole),
-        cost_estimate=cost(8_000_000_000, 8_000_000),
-        compiler_params=room(16),
-        name="write",
-    )(lengths, accepted, gathered, cache_keys, cache_values)
     normed = pl.pallas_call(
         finish_kernel,
-        out_shape=shape((N_KV, PROP, LANES)),
+        out_shape=near((N_KV, PROP, LANES)),
         in_specs=[smem(), vmem(), vmem(), vmem()],
         out_specs=vmem(),
         compiler_params=room(8),
@@ -308,7 +385,7 @@
     arrived_normed = exchange(normed, "kv")
     partial_out = pl.pallas_call(
         output_kernel,
-        out_shape=shape((N_TP, SEQS * PROP, w_output.shape[1])),
+        out_shape=near((N_TP, SEQS * PROP, w_output.shape[1])),
         in_specs=[vmem(), vmem()],
         out_specs=vmem(),
         compiler_params=room(8),

time: 81.3 us -> 75.5 us (0.929)
  blocking collectives: 36.7 us -> 64.8 us
  starting transfers between devices: 13.4 us -> 0 us
  waiting for transfers between devices: 9.5 us -> 0 us
  local copies, waits for them, and re-layouts: 7.68 us -> 0.04 us
  Pallas kernels: 12.6 us -> 9.54 us
    all_to_all x0 -> x2, blocking collectives: none -> 28.1 us  [the longest x1 18 us: local(): arrived_out = exchange(partial_out, 'tp')]
    all_to_all x2 -> x0, starting transfers between devices: 13.4 us -> none  [the longest x1 9.92 us: local(): arrived_out = exchange(partial_out, 'tp')]
    all_to_all x2 -> x0, waiting for transfers between devices: 9.5 us -> none  [the longest x1 6.36 us: local(): arrived_parts = exchange(parts, 'kv')]
    unnamed x28 -> x14, local copies, waits for them, and re-layouts: 7.68 us -> 0.04 us
    pallas_call x7 -> x5, Pallas kernels: 11.9 us -> 8.87 us  [the longest x1 5.7 us: local(): pl.pallas_call(attend_kernel, out_shape=(near((N_KV, 56, LANES)), shape(c...]
  transfers between devices with their start and end apart: 2 -> 0, of which waited for: 2 -> 0; matrix products, arithmetic and copies ran while one was open for 0% -> 0% of each run, Pallas kernels for 5% -> 0%
where the time goes in v2:
time: 75.5 us; the launch traced here: 75.2 us
  blocking collectives  64.8 us (86%)
  Pallas kernels  9.54 us (13%)
    all_to_all x1, blocking collectives, local(): arrived_out = exchange(partial_out, 'tp')  18 us
    all_to_all x1, blocking collectives, local(): arrived = exchange(partial, 'kv')  16.7 us
    all_to_all x1, blocking collectives, local(): gathered = exchange(copies, 'kv')  10.7 us
    all_to_all x1, blocking collectives, local(): arrived_parts = exchange(parts, 'kv')  10.1 us
    all_to_all x1, blocking collectives, local(): arrived_normed = exchange(normed, 'kv')  9.33 us
    pallas_call x1, Pallas kernels, local(): pl.pallas_call(attend_kernel, out_shape=(near((N_KV, 56, LANES)), shape(c...  5.7 us
    pallas_call x1, Pallas kernels, local(): pl.pallas_call(project_kernel, out_shape=near((N_KV, 80, LANES)), in_spec...  1.73 us

profile of v2, /device:TPU:1, one launch (start us, length us, event | category | flops | bytes accessed | tf_op | source)
XLA Modules:
  0.0 75.2 jit_solution(14983876217488180195)
XLA Ops:
  0.6 0.0 copy-start.5
  0.6 0.0 copy-start.4
  0.7 0.0 copy-start.2
  0.7 0.0 copy-start
  0.7 1.7 %project.1 = bf16[16,80,128]{2,1,0:T(8,128)(2,1)S(1)} custom-call(bf16[96,256]{1,0:T(8,128)(2,1)} %tokens_far.1, f32[1,256]{1,0:T(1,128)} %bitcast.3, bf16[256,512]{1,0:T(8,128)(2,1)} %query_far.1, bf16[256,512]{1,0:T(8,128)(2,1)} %key_far.1, bf16[256,512]{1,0:T(8,128)(2,1)} %value_far.1), custom_call_target="tpu_custom_call" | custom-call | tf_op jit(solution)/shard_map/project/pallas_call | solution.py:329
  2.4 16.7 %all_to_all.25.arrived = bf16[16,80,128]{2,1,0:T(8,128)(2,1)S(1)} all-to-all(bf16[16,80,128]{2,1,0:T(8,128)(2,1)S(1)} %project.1), channel_id=1, replica_groups=mesh['kv'=16,'tp'=8] {'kv'}, dimensions={0} | all-to-all | bytes 655360 | tf_op jit(solution)/shard_map/all_to_all | solution.py:346
  19.2 0.1 normalize.1
  19.3 10.7 %all_to_all.26.gathered = bf16[16,72,128]{2,1,0:T(8,128)(2,1)S(1)} all-to-all(bf16[16,72,128]{2,1,0:T(8,128)(2,1)S(1)} %get-tuple-element.9), channel_id=1, replica_groups=mesh['kv'=16,'tp'=8] {'kv'}, dimensions={0} | all-to-all | bytes 589824 | tf_op jit(solution)/shard_map/all_to_all | solution.py:355
  30.0 0.0 copy-done.5
  30.0 0.0 copy-done.4
  30.0 0.0 copy-done.2
  30.0 0.0 copy-done
  30.0 0.0 copy-start.3
  30.0 0.0 copy-start.6
  30.0 0.0 copy-start.1
  30.0 5.7 %attend.1 = (bf16[16,56,128]{2,1,0:T(8,128)(2,1)S(1)}, bf16[4,512,512]{2,1,0:T(8,128)(2,1)}, bf16[4,512,512]{2,1,0:T(8,128)(2,1)}, f32[56,128]{1,0:T(8,128)S(1)}) custom-call(s32[4]{0:T(128)S(1)} %copy-done.4, s32[4]{0:T(128)S(1)} %copy-done.5, bf16[16,72,128]{2,1,0:T(8,128)(2,1)S(1)} %all_to_all.26.gathered, bf16[4,512,512]{2,1,0:T(8,128)(2,1)S(1)} %copy-done, ...), custom_call_target="tpu_custom_call" | custom-call | tf_op jit(solution)/shard_map/attend/pallas_call | solution.py:356
  35.7 10.1 %all_to_all.27.arrived = bf16[16,56,128]{2,1,0:T(8,128)(2,1)S(1)} all-to-all(bf16[16,56,128]{2,1,0:T(8,128)(2,1)S(1)} %get-tuple-element.11), channel_id=1, replica_groups=mesh['kv'=16,'tp'=8] {'kv'}, dimensions={0} | all-to-all | bytes 458752 | tf_op jit(solution)/shard_map/all_to_all | solution.py:376
  45.8 0.0 copy-done.3
  45.8 1.1 %finish.1 = bf16[16,24,128]{2,1,0:T(8,128)(2,1)S(1)} custom-call(f32[8]{0:T(128)S(1)} %copy-done.6, f32[4,128]{1,0:T(4,128)S(1)} %bitcast.2, bf16[16,56,128]{2,1,0:T(8,128)(2,1)S(1)} %all_to_all.27.arrived, f32[56,128]{1,0:T(8,128)S(1)} %get-tuple-element.12.own_part), custom_call_target="tpu_custom_call" | custom-call | tf_op jit(solution)/shard_map/finish/pallas_call | solution.py:377
  46.9 9.3 %all_to_all.28.arrived = bf16[16,24,128]{2,1,0:T(8,128)(2,1)S(1)} all-to-all(bf16[16,24,128]{2,1,0:T(8,128)(2,1)S(1)} %finish.1), channel_id=1, replica_groups=mesh['kv'=16,'tp'=8] {'kv'}, dimensions={0} | all-to-all | bytes 196608 | tf_op jit(solution)/shard_map/all_to_all | solution.py:385
  56.3 0.0 copy-done.1
  56.3 0.2 output.1
  56.5 18.0 %all_to_all.29.arrived = bf16[8,96,256]{2,1,0:T(8,128)(2,1)S(1)} all-to-all(bf16[8,96,256]{2,1,0:T(8,128)(2,1)S(1)} %output.1), channel_id=1, replica_groups=mesh['kv'=16,'tp'=8] {'tp'}, dimensions={0} | all-to-all | bytes 786432 | tf_op jit(solution)/shard_map/all_to_all | solution.py:394
  74.5 0.7 mix.1
  (1 shorter events, 0.0 us)
Async XLA Ops:
  0.6 29.3 %copy-start.5 = (s32[4]{0:T(128)S(1)}, s32[4]{0:T(128)}, u32[]{:S(2)}) copy-start(s32[4]{0:T(128)} %accepted.1) | copy-start | bytes 52
  0.6 29.3 %copy-start.4 = (s32[4]{0:T(128)S(1)}, s32[4]{0:T(128)}, u32[]{:S(2)}) copy-start(s32[4]{0:T(128)} %lengths.1) | copy-start | bytes 52
  0.7 29.3 %copy-start.2 = (s32[4,24]{1,0:T(4,128)S(1)}, s32[4,24]{1,0:T(4,128)}, u32[]{:S(2)}) copy-start(s32[4,24]{1,0:T(4,128)} %parents.1) | copy-start | bytes 1156
  0.7 29.3 %copy-start = (bf16[4,512,512]{2,1,0:T(8,128)(2,1)S(1)}, bf16[4,512,512]{2,1,0:T(8,128)(2,1)}, u32[]{:S(2)}) copy-start(bf16[4,512,512]{2,1,0:T(8,128)(2,1)} %keys.1) | copy-start | bytes 6291460
  30.0 15.8 %copy-start.3 = (f32[512]{0:T(512)S(1)}, f32[512]{0:T(512)}, u32[]{:S(2)}) copy-start(f32[512]{0:T(512)} %param.22) | copy-start | bytes 6148
  30.0 15.8 %copy-start.6 = (f32[8]{0:T(128)S(1)}, f32[8]{0:T(128)}, u32[]{:S(2)}) copy-start(f32[8]{0:T(128)} %map_lambda.1) | copy-start | bytes 100
  30.0 26.2 %copy-start.1 = (bf16[512,256]{1,0:T(8,128)(2,1)S(1)}, bf16[512,256]{1,0:T(8,128)(2,1)}, u32[]{:S(2)}) copy-start(bf16[512,256]{1,0:T(8,128)(2,1)} %w_output.1) | copy-start | bytes 786436

commit v3 on v2

v3 whole, which is shorter than its diff:
```python
import functools

import jax
import jax.numpy as jnp
from jax import lax
from jax.experimental import pallas as pl
from jax.experimental.pallas import tpu as pltpu
from jax.sharding import PartitionSpec as P

D = 4096
HEAD = 64
QK = 32
SEQS = 4
PROP = 24
PAIRS = 4
LANES = 128
N_KV = 16
N_TP = 8
WINDOW = 48
LAG = 3

f32 = jnp.float32
bf16 = jnp.bfloat16
epsilon = 1e-05
masked_low = -1e30
score_scale = QK ** (-0.5)
LOG2E = 1.4426950408889634

NT = (((1,), (1,)), ((), ()))
NN = (((1,), (0,)), ((), ()))


def iota(shape, dim):
    return lax.broadcasted_iota(jnp.int32, shape, dim)


def three_parts(first, second):
    place = iota((8, LANES), 0)
    wide = jnp.where(place % 2 == 0, first, second)
    high = wide.astype(bf16).astype(f32)
    rest = wide - high
    middle = rest.astype(bf16).astype(f32)
    low = rest - middle
    tile = jnp.where(place < 2, high, jnp.where(place < 4, middle, jnp.where(place < 6, low, 0.0)))
    return tile.astype(bf16)


def column_to_row(column):
    count = column.shape[0]
    eye = iota((count, LANES), 0) == iota((count, LANES), 1)
    return jnp.sum(jnp.where(eye, column, 0.0), axis=0, keepdims=True)


def row_to_column(row, count):
    eye = iota((count, LANES), 0) == iota((count, LANES), 1)
    return jnp.sum(jnp.where(eye, row, 0.0), axis=1, keepdims=True)


def project_kernel(
    tokens_far,
    gain_far,
    query_far,
    key_far,
    value_far,
    out,
    tokens,
    gain,
    query,
    key,
    value,
    done,
):
    far = (tokens_far, gain_far, query_far, key_far, value_far)
    near = (tokens, gain, query, key, value)
    loads = [pltpu.make_async_copy(a, b, done.at[place]) for place, (a, b) in enumerate(zip(far, near))]
    for load in loads:
        load.start()
    for load in loads[:2]:
        load.wait()
    wide = tokens[...].astype(f32)
    gained = (wide * gain[...]).astype(bf16)
    squares = jnp.sum(wide * wide, axis=1, keepdims=True)
    for seq in range(SEQS):
        row = column_to_row(squares[seq * PROP : (seq + 1) * PROP])
        tile = three_parts(row, row)
        for pair in range(PAIRS):
            out[seq * PAIRS + pair, 3 * PROP :, :] = tile
    for place, weight in enumerate((query, key, value)):
        loads[2 + place].wait()
        product = lax.dot_general(gained, weight[...], NN, preferred_element_type=f32).astype(bf16)
        for seq in range(SEQS):
            for pair in range(PAIRS):
                out[seq * PAIRS + pair, place * PROP : (place + 1) * PROP, :] = product[
                    seq * PROP : (seq + 1) * PROP, pair * LANES : (pair + 1) * LANES
                ]


def normalize_kernel(arrived, own, copies):
    total = arrived[0].astype(f32)
    for source in range(1, N_KV):
        total = total + arrived[source].astype(f32)
    row = total[72:73] + total[74:75] + total[76:77]
    factor = lax.rsqrt(row_to_column(row, PROP) / D + epsilon)
    for place in range(3):
        rows = slice(place * PROP, (place + 1) * PROP)
        scaled = factor * (score_scale * LOG2E) if place == 0 else factor
        part = (total[rows] * scaled).astype(bf16)
        own[rows, :] = part
        for target in range(N_KV):
            copies[target, rows, :] = part


def expanded(queries):
    group = iota(queries.shape, 1) // QK
    zero = jnp.zeros_like(queries)
    return jnp.concatenate([jnp.where(group == place, queries, zero) for place in range(4)], axis=0)


def by_head(array):
    return jnp.where(iota((48, LANES), 1) < HEAD, array[:48], array[48:])


def own_steps(parents, own, out):
    eye = iota((PROP, PROP), 0) == iota((PROP, PROP), 1)
    links = parents[pl.ds(lax.axis_index("kv") // PAIRS, 1), :].astype(f32)
    column = jnp.sum(jnp.where(eye, links, 0.0), axis=1, keepdims=True)
    reached = jnp.where(eye | (column == iota((PROP, PROP), 1).astype(f32)), 1.0, 0.0)
    queries, keys, values = own[:PROP, :], own[PROP : 2 * PROP, :], own[2 * PROP :, :]
    scores = lax.dot_general(expanded(queries), keys, NT, preferred_element_type=f32)
    yield
    for _ in range(5):
        narrow = reached.astype(bf16)
        reached = jnp.minimum(1.0, lax.dot_general(narrow, narrow, NN, preferred_element_type=f32))
        yield
    related = jnp.concatenate([reached] * 4, axis=0) > 0.5
    scores = jnp.where(related, scores, masked_low)
    largest = jnp.max(scores, axis=1, keepdims=True)
    yield
    weight = jnp.where(related, jnp.exp2(scores - largest), 0.0)
    total = jnp.sum(weight, axis=1, keepdims=True)
    yield
    product = lax.dot_general(weight.astype(bf16), values, NN, preferred_element_type=f32)
    yield
    out[:48, :] = by_head(product / total)
    out[48:, :] = by_head(jnp.broadcast_to(largest + jnp.log2(total), (96, LANES)))
    yield


def attend_kernel(
    lengths,
    accepted,
    gathered,
    keys,
    values,
    out_far,
    out,
    sent,
):
    block_len = keys.shape[1]
    ends = lengths[...] + accepted[...] - lax.axis_index("kv") * block_len
    sends = [
        pltpu.make_async_copy(
            out.at[pl.ds(seq * PAIRS, PAIRS)], out_far.at[pl.ds(seq * PAIRS, PAIRS)], sent.at[seq]
        )
        for seq in range(SEQS)
    ]
    def scored(seq, pair):
        lanes = slice(pair * LANES, (pair + 1) * LANES)
        queries = expanded(gathered[seq * PAIRS + pair, :PROP, :])
        return lax.dot_general(queries, keys[seq, :, lanes], NT, preferred_element_type=f32)

    def weighed(seq, scores):
        visible = iota((1, block_len), 1) < ends[:, seq : seq + 1]
        scores = jnp.where(visible, scores, masked_low)
        largest = jnp.max(scores, axis=1, keepdims=True)
        return largest, jnp.exp2(scores - largest).astype(bf16)

    ones = jnp.ones((block_len, LANES), bf16)
    eye = iota((48, LANES), 0) == iota((48, LANES), 1)

    def finished(seq, pair, largest, weight):
        lanes = slice(pair * LANES, (pair + 1) * LANES)
        both = jnp.concatenate([values[seq, :, lanes], ones], axis=1)
        product = lax.dot_general(weight, both, NN, preferred_element_type=f32)
        total = product[:, LANES:]
        out[seq * PAIRS + pair, :48, :] = by_head(product[:, :LANES] / total).astype(bf16)
        level = largest + jnp.log2(total)
        first = jnp.sum(jnp.where(eye, level[:48], 0.0), axis=0, keepdims=True)
        second = jnp.sum(jnp.where(eye, level[48:], 0.0), axis=0, keepdims=True)
        seen = ends[:, seq : seq + 1] > 0
        tile = three_parts(jnp.where(seen, first, masked_low), jnp.where(seen, second, masked_low))
        out[seq * PAIRS + pair, 48:, :] = tile

    units = [(seq, pair) for seq in range(SEQS) for pair in range(PAIRS)]
    scores = scored(*units[0])
    waiting = []
    for place in range(len(units) + LAG):
        if place < len(units):
            following = scored(*units[place + 1]) if place + 1 < len(units) else None
            waiting.append((units[place], weighed(units[place][0], scores)))
            scores = following
        if place >= LAG:
            (seq, pair), found = waiting.pop(0)
            finished(seq, pair, *found)
            if pair == PAIRS - 1:
                sends[seq].start()
    for send in sends:
        send.wait()


def write_kernel(
    lengths,
    accepted,
    gathered,
    parents,
    own,
    keys_far,
    values_far,
    new_keys,
    new_values,
    own_part,
    keys,
    values,
    window,
    loaded,
    stored,
    patched,
):
    block_len = keys.shape[1]
    offset = lax.axis_index("kv") * block_len
    pieces = [
        (seq, place, source, middle, target)
        for seq in range(SEQS)
        for place, (source, middle, target) in enumerate(
            ((keys_far, keys, new_keys), (values_far, values, new_values))
        )
    ]
    loads = [pltpu.make_async_copy(a.at[seq], b.at[seq], loaded.at[seq, place]) for seq, place, a, b, _ in pieces]
    stores = [pltpu.make_async_copy(b.at[seq], c.at[seq], stored.at[seq, place]) for seq, place, _, b, c in pieces]
    for load in loads:
        load.start()
    for _ in own_steps(parents, own, own_part):
        pass
    for load, store in zip(loads, stores):
        load.wait()
        store.start()

    def patch(seq):
        begin = lengths[seq] + accepted[seq] - offset
        base = pl.multiple_of(jnp.clip((begin // 16) * 16, 0, block_len - WINDOW), 16)
        copies = [
            pltpu.make_async_copy(
                window.at[seq, place], target.at[seq, pl.ds(base, WINDOW)], patched.at[seq, place]
            )
            for place, target in enumerate((new_keys, new_values))
        ]
        here = (begin > -PROP) & (begin < block_len)

        @pl.when(here)
        def _():
            shift = base - begin
            placing = (shift + iota((WINDOW, PROP), 0) == iota((WINDOW, PROP), 1)).astype(bf16)
            row = shift + iota((WINDOW, PAIRS * LANES), 0)
            written = (row >= 0) & (row < PROP)
            for place, source in ((0, keys), (1, values)):
                rows = jnp.concatenate(
                    [
                        gathered[seq * PAIRS + pair, (place + 1) * PROP : (place + 2) * PROP, :]
                        for pair in range(PAIRS)
                    ],
                    axis=1,
                )
                moved = lax.dot_general(placing, rows, NN, preferred_element_type=f32)
                old = source[seq, pl.ds(base, WINDOW), :].astype(f32)
                window[seq, place] = jnp.where(written, moved, old).astype(bf16)
            for place in range(2):
                stores[2 * seq + place].wait()
                copies[place].start()

        @pl.when(jnp.logical_not(here))
        def _():
            for place in range(2):
                stores[2 * seq + place].wait()

        return here, copies

    for here, copies in [patch(seq) for seq in range(SEQS)]:

        @pl.when(here)
        def _():
            for copy in copies:
                copy.wait()


def finish_kernel(map_lambda, out_gain, arrived, own_part, copies):
    pair = lax.axis_index("kv") % PAIRS
    lane = iota((48, LANES), 1)
    levels = jnp.concatenate([arrived[source, 48:, :].astype(f32) for source in range(N_KV)], axis=0).T[:48]
    levels = levels + pltpu.roll(levels, LANES - 2, 1) + pltpu.roll(levels, LANES - 4, 1)
    own_level = own_part[48:, :]
    is_first, is_second = lane % 8 == 0, lane % 8 == 1
    top = [
        jnp.maximum(
            jnp.max(jnp.where(mine, levels, masked_low), axis=1, keepdims=True), own_level[:, spot : spot + 1]
        )
        for mine, spot in ((is_first, 0), (is_second, HEAD))
    ]
    weights = jnp.exp2(jnp.where(is_first, levels - top[0], jnp.where(is_second, levels - top[1], masked_low)))
    own_weight = jnp.exp2(own_level - jnp.where(lane < HEAD, top[0], top[1]))
    sums = [jnp.sum(jnp.where(mine, weights, 0.0), axis=1, keepdims=True) for mine in (is_first, is_second)]
    whole = jnp.where(lane < HEAD, sums[0], sums[1]) + own_weight
    total = own_weight * own_part[:48, :]
    spot = jnp.where(lane < HEAD, 0, 1)
    for source in range(N_KV):
        factor = jnp.take_along_axis(weights, spot + 8 * source, axis=1, mode="promise_in_bounds")
        total = total + factor * arrived[source, :48, :].astype(f32)
    total = total / whole
    lane_first = iota((PROP, LANES), 1) < HEAD
    heads = iota((1, 8), 1) - 2 * pair
    lams = [jnp.sum(jnp.where(heads == head, map_lambda[...], 0.0), axis=1, keepdims=True) for head in (0, 1)]
    lam = jnp.where(lane_first, lams[0], lams[1])
    difference = total[:PROP] - lam * total[PROP:]
    squared = difference * difference
    mean_first = jnp.sum(jnp.where(lane_first, squared, 0.0), axis=1, keepdims=True)
    mean_second = jnp.sum(jnp.where(lane_first, 0.0, squared), axis=1, keepdims=True)
    mean = jnp.where(lane_first, mean_first, mean_second) / HEAD
    normed = (difference * lax.rsqrt(mean + epsilon) * out_gain[pl.ds(pair, 1), :]).astype(bf16)
    for target in range(N_KV):
        copies[target] = normed


def output_kernel(arrived, w_output, copies):
    total = None
    for pair in range(PAIRS):
        rows = jnp.concatenate([arrived[seq * PAIRS + pair] for seq in range(SEQS)], axis=0)
        part = lax.dot_general(
            rows, w_output[pair * LANES : (pair + 1) * LANES, :], NN, preferred_element_type=f32
        )
        total = part if total is None else total + part
    total = total.astype(bf16)
    for target in range(N_TP):
        copies[target] = total


def mix_kernel(arrived, out):
    total = arrived[0].astype(f32)
    for source in range(1, N_TP):
        total = total + arrived[source].astype(f32)
    out[...] = total.astype(bf16)


def vmem():
    return pl.BlockSpec(memory_space=pltpu.VMEM)


def hbm():
    return pl.BlockSpec(memory_space=pltpu.HBM)


def smem():
    return pl.BlockSpec(memory_space=pltpu.SMEM)


def shape(dims, kind=bf16):
    return jax.ShapeDtypeStruct(dims, kind)


def room(mebibytes):
    return pltpu.CompilerParams(vmem_limit_bytes=mebibytes * 1024 * 1024)


def near(dims, kind=bf16):
    return pltpu.VMEM(dims, kind)


def far(*arrays):
    return [pltpu.with_memory_space_constraint(array, pltpu.HBM) for array in arrays]


def cost(flops, moved):
    return pl.CostEstimate(flops=flops, bytes_accessed=moved, transcendentals=0)


def local(
    tokens,
    norm_gain,
    w_query,
    w_key,
    w_value,
    w_output,
    cache_keys,
    cache_values,
    map_lambda,
    out_gain,
    parents,
    lengths,
    accepted,
):
    width = cache_keys.shape[2]
    exchange = functools.partial(lax.all_to_all, split_axis=0, concat_axis=0, tiled=True)

    partial = pl.pallas_call(
        project_kernel,
        out_shape=near((N_KV, 80, LANES)),
        in_specs=[hbm()] * 5,
        out_specs=vmem(),
        scratch_shapes=[
            pltpu.VMEM(tokens.shape, bf16),
            pltpu.VMEM((1, norm_gain.shape[0]), f32),
            pltpu.VMEM(w_query.shape, bf16),
            pltpu.VMEM(w_key.shape, bf16),
            pltpu.VMEM(w_value.shape, bf16),
            pltpu.SemaphoreType.DMA((5,)),
        ],
        compiler_params=room(8),
        cost_estimate=cost(20_000_000_000, 40_000_000),
        name="project",
    )(*far(tokens, norm_gain.reshape(1, -1), w_query, w_key, w_value))
    near_keys = pltpu.with_memory_space_constraint(cache_keys, pltpu.VMEM)
    near_values = pltpu.with_memory_space_constraint(cache_values, pltpu.VMEM)
    arrived = exchange(partial, "kv")
    own, copies = pl.pallas_call(
        normalize_kernel,
        out_shape=(near((72, LANES)), near((N_KV, 72, LANES))),
        in_specs=[vmem()],
        out_specs=(vmem(), vmem()),
        compiler_params=room(8),
        cost_estimate=cost(20_000_000_000, 40_000_000),
        name="normalize",
    )(arrived)
    gathered = exchange(copies, "kv")
    parts = pl.pallas_call(
        attend_kernel,
        out_shape=shape((N_KV, 56, LANES)),
        in_specs=[vmem()] * 5,
        out_specs=hbm(),
        scratch_shapes=[
            pltpu.VMEM((N_KV, 56, LANES), bf16),
            pltpu.SemaphoreType.DMA((SEQS,)),
        ],
        compiler_params=room(24),
        name="attend",
    )(lengths.reshape(1, -1), accepted.reshape(1, -1), gathered, near_keys, near_values)
    arrived_parts = exchange(parts, "kv")
    new_keys, new_values, own_part = pl.pallas_call(
        write_kernel,
        out_shape=(shape(cache_keys.shape), shape(cache_values.shape), near((96, LANES), f32)),
        in_specs=[smem(), smem()] + [vmem()] * 3 + [hbm(), hbm()],
        out_specs=(hbm(), hbm(), vmem()),
        scratch_shapes=[
            pltpu.VMEM(cache_keys.shape, bf16),
            pltpu.VMEM(cache_values.shape, bf16),
            pltpu.VMEM((SEQS, 2, WINDOW, width), bf16),
            pltpu.SemaphoreType.DMA((SEQS, 2)),
            pltpu.SemaphoreType.DMA((SEQS, 2)),
            pltpu.SemaphoreType.DMA((SEQS, 2)),
        ],
        compiler_params=room(24),
        cost_estimate=cost(8_000_000_000, 8_000_000),
        name="write",
    )(lengths, accepted, gathered, parents, own, *far(cache_keys, cache_values))
    normed = pl.pallas_call(
        finish_kernel,
        out_shape=near((N_KV, PROP, LANES)),
        in_specs=[vmem()] * 4,
        out_specs=vmem(),
        compiler_params=room(8),
        name="finish",
    )(map_lambda.reshape(1, -1), out_gain.reshape(PAIRS, LANES), arrived_parts, own_part)
    arrived_normed = exchange(normed, "kv")
    partial_out = pl.pallas_call(
        output_kernel,
        out_shape=near((N_TP, SEQS * PROP, w_output.shape[1])),
        in_specs=[vmem(), vmem()],
        out_specs=vmem(),
        compiler_params=room(8),
        name="output",
    )(arrived_normed, w_output)
    arrived_out = exchange(partial_out, "tp")
    mixed = pl.pallas_call(
        mix_kernel,
        out_shape=shape((SEQS * PROP, w_output.shape[1])),
        in_specs=[vmem()],
        out_specs=vmem(),
        compiler_params=room(8),
        name="mix",
    )(arrived_out)
    return (mixed, new_keys, new_values)


def solution(mesh):
    return jax.shard_map(
        local,
        mesh=mesh,
        in_specs=(
            P(None, "kv"),
            P("kv"),
            P("kv", "tp"),
            P("kv", "tp"),
            P("kv", "tp"),
            P("tp", "kv"),
            P(None, "kv", "tp"),
            P(None, "kv", "tp"),
            P("tp"),
            P("tp"),
            P(),
            P(),
            P(),
        ),
        out_specs=(P(None, "kv"), P(None, "kv", "tp"), P(None, "kv", "tp")),
        check_vma=False,
    )
```

time: 75.5 us -> 73 us (0.967)
  blocking collectives: 64.8 us -> 55.3 us
  starting transfers between devices: 0 us -> 3.54 us
  waiting for transfers between devices: 0 us -> 2.38 us
  Pallas kernels: 9.54 us -> 10.6 us
    all_to_all x1 -> x0, blocking collectives: 10.1 us -> none  [local(): arrived_parts = exchange(parts, 'kv')]
    all_to_all x0 -> x1, starting transfers between devices: none -> 3.54 us  [local(): arrived_parts = exchange(parts, 'kv')]
    all_to_all x0 -> x1, waiting for transfers between devices: none -> 2.38 us  [local(): arrived_parts = exchange(parts, 'kv')]
    pallas_call x1 -> x2, Pallas kernels: 5.7 us -> 7.19 us  [the longest x1 4.9 us: local(): pl.pallas_call(write_kernel, out_shape=(shape(cache_keys.shape), shape(ca...]
    all_to_all x1, blocking collectives: 9.33 us -> 10.8 us  [local(): arrived_normed = exchange(normed, 'kv')]
    all_to_all x1, blocking collectives: 18 us -> 16.9 us  [local(): arrived_out = exchange(partial_out, 'tp')]
  transfers between devices with their start and end apart: 0 -> 1, of which waited for: 0 -> 1; matrix products, arithmetic and copies ran while one was open for 0% -> 0% of each run, Pallas kernels for 0% -> 7%
where the time goes in v3:
time: 73 us; the launch traced here: 72.6 us
  blocking collectives  55.3 us (76%)
  Pallas kernels  10.6 us (15%)
  starting transfers between devices  3.54 us (5%)
  waiting for transfers between devices  2.38 us (3%)
  between operations  0.75 us (1%)
    all_to_all x1, blocking collectives, local(): arrived_out = exchange(partial_out, 'tp')  16.9 us
    all_to_all x1, blocking collectives, local(): arrived = exchange(partial, 'kv')  16.7 us
    all_to_all x1, blocking collectives, local(): gathered = exchange(copies, 'kv')  10.9 us
    all_to_all x1, blocking collectives, local(): arrived_normed = exchange(normed, 'kv')  10.8 us
    pallas_call x1, Pallas kernels, local(): pl.pallas_call(write_kernel, out_shape=(shape(cache_keys.shape), shape(ca...  4.9 us
    all_to_all x1, starting transfers between devices, local(): arrived_parts = exchange(parts, 'kv')  3.54 us
    all_to_all x1, waiting for transfers between devices, local(): arrived_parts = exchange(parts, 'kv')  2.38 us
    pallas_call x1, Pallas kernels, local(): pl.pallas_call(attend_kernel, out_shape=shape((N_KV, 56, LANES)), in_spec...  2.29 us
  transfers between devices with their start and end apart: 1, of which 1 were waited for; matrix products, arithmetic and copies ran while one was open for 0% of the time, Pallas kernels for 7%

profile of v3, /device:TPU:1, one launch (start us, length us, event | category | flops | bytes accessed | tf_op | source)
XLA Modules:
  0.0 72.6 jit_solution(16634526630259049735)
XLA Ops:
  0.6 1.6 %project.1 = bf16[16,80,128]{2,1,0:T(8,128)(2,1)S(1)} custom-call(bf16[96,256]{1,0:T(8,128)(2,1)} %tokens_far.1, f32[1,256]{1,0:T(1,128)} %bitcast.9, bf16[256,512]{1,0:T(8,128)(2,1)} %query_far.1, bf16[256,512]{1,0:T(8,128)(2,1)} %key_far.1, bf16[256,512]{1,0:T(8,128)(2,1)} %value_far.1), custom_call_target="tpu_custom_call" | custom-call | flops 20000000000 | bytes 40000000 | tf_op jit(solution)/shard_map/project/pallas_call | solution.py:402
  2.2 16.7 %all_to_all.25.arrived = bf16[16,80,128]{2,1,0:T(8,128)(2,1)S(1)} all-to-all(bf16[16,80,128]{2,1,0:T(8,128)(2,1)S(1)} %project.1), channel_id=1, replica_groups=mesh['kv'=16,'tp'=8] {'kv'}, dimensions={0} | all-to-all | bytes 655360 | tf_op jit(solution)/shard_map/all_to_all | solution.py:421
  19.0 0.1 normalize.1
  19.1 10.9 %all_to_all.26.gathered = bf16[16,72,128]{2,1,0:T(8,128)(2,1)S(1)} all-to-all(bf16[16,72,128]{2,1,0:T(8,128)(2,1)S(1)} %get-tuple-element.8), channel_id=1, replica_groups=mesh['kv'=16,'tp'=8] {'kv'}, dimensions={0} | all-to-all | bytes 589824 | tf_op jit(solution)/shard_map/all_to_all | solution.py:431
  30.1 0.0 copy-done
  30.1 0.0 copy-done.1
  30.1 0.0 copy-done.4
  30.1 0.0 copy-done.5
  30.1 0.0 copy-start.7
  30.1 2.3 %attend.1 = bf16[16,56,128]{2,1,0:T(8,128)(2,1)} custom-call(s32[1,4]{1,0:T(1,128)S(1)} %bitcast.6, s32[1,4]{1,0:T(1,128)S(1)} %bitcast.7, bf16[16,72,128]{2,1,0:T(8,128)(2,1)S(1)} %all_to_all.26.gathered, bf16[4,512,512]{2,1,0:T(8,128)(2,1)S(1)} %copy-done, bf16[4,512,512]{2,1,0:T(8,128)(2,1)S(1)} %copy-done.1), custom_call_target="tpu_custom_call" | custom-call | tf_op jit(solution)/shard_map/attend/pallas_call | solution.py:432
  32.4 3.5 %all-to-all-start.2 = ((bf16[16,56,128]{2,1,0:T(8,128)(2,1)}), bf16[16,56,128]{2,1,0:T(8,128)(2,1)S(1)}, u32[]{:S(2)}, u32[]{:S(2)}) async-start(bf16[16,56,128]{2,1,0:T(8,128)(2,1)} %attend.1), calls=%async_computation.2 | async-start | bytes 458752 | tf_op jit(solution)/shard_map/all_to_all | solution.py:444
  35.9 0.0 copy-done.7
  35.9 0.0 copy-start.3
  36.0 0.0 copy-start.6
  36.0 0.0 copy-start.2
  36.0 4.9 %write.1 = (bf16[4,512,512]{2,1,0:T(8,128)(2,1)}, bf16[4,512,512]{2,1,0:T(8,128)(2,1)}, f32[96,128]{1,0:T(8,128)S(1)}) custom-call(s32[4]{0:T(128)S(1)} %copy-done.4, s32[4]{0:T(128)S(1)} %copy-done.5, bf16[16,72,128]{2,1,0:T(8,128)(2,1)S(1)} %all_to_all.26.gathered, s32[4,24]{1,0:T(4,128)S(1)} %copy-done.7, bf16[72,128]{1,0:T(8,128)(2,1)S(1)} %get-tuple-element.9.own, ...), custom_call_target="tpu_custom_call" | custom-call | flops 8000000000 | bytes 8000000 | tf_op jit(solution)/shard_map/write/pallas_call | solution.py:445
  40.9 2.4 %all-to-all-done.2.arrived = bf16[16,56,128]{2,1,0:T(8,128)(2,1)S(1)} async-done(((bf16[16,56,128]{2,1,0:T(8,128)(2,1)}), bf16[16,56,128]{2,1,0:T(8,128)(2,1)S(1)}, u32[]{:S(2)}, u32[]{:S(2)}) %all-to-all-start.2) | async-done | bytes 229408 | tf_op jit(solution)/shard_map/all_to_all | solution.py:444
  43.3 0.0 copy-done.3
  43.3 0.0 copy-done.6
  43.3 0.8 %finish.1 = bf16[16,24,128]{2,1,0:T(8,128)(2,1)S(1)} custom-call(f32[1,8]{1,0:T(1,128)S(1)} %bitcast.8, f32[4,128]{1,0:T(4,128)S(1)} %bitcast.5, bf16[16,56,128]{2,1,0:T(8,128)(2,1)S(1)} %all-to-all-done.2.arrived, f32[96,128]{1,0:T(8,128)S(1)} %get-tuple-element.10.own_part), custom_call_target="tpu_custom_call" | custom-call | tf_op jit(solution)/shard_map/finish/pallas_call | solution.py:462
  44.1 10.8 %all_to_all.27.arrived = bf16[16,24,128]{2,1,0:T(8,128)(2,1)S(1)} all-to-all(bf16[16,24,128]{2,1,0:T(8,128)(2,1)S(1)} %finish.1), channel_id=1, replica_groups=mesh['kv'=16,'tp'=8] {'kv'}, dimensions={0} | all-to-all | bytes 196608 | tf_op jit(solution)/shard_map/all_to_all | solution.py:470
  54.9 0.2 output.1
  55.1 16.9 %all_to_all.28.arrived = bf16[8,96,256]{2,1,0:T(8,128)(2,1)S(1)} all-to-all(bf16[8,96,256]{2,1,0:T(8,128)(2,1)S(1)} %output.1), channel_id=1, replica_groups=mesh['kv'=16,'tp'=8] {'tp'}, dimensions={0} | all-to-all | bytes 786432 | tf_op jit(solution)/shard_map/all_to_all | solution.py:479
  71.9 0.7 mix.1
  (5 shorter events, 0.0 us)
Async XLA Ops:
  19.0 11.1 %copy-start = (bf16[4,512,512]{2,1,0:T(8,128)(2,1)S(1)}, bf16[4,512,512]{2,1,0:T(8,128)(2,1)}, u32[]{:S(2)}) copy-start(bf16[4,512,512]{2,1,0:T(8,128)(2,1)} %keys_far.1) | copy-start | bytes 6291460
  19.0 11.1 %copy-start.1 = (bf16[4,512,512]{2,1,0:T(8,128)(2,1)S(1)}, bf16[4,512,512]{2,1,0:T(8,128)(2,1)}, u32[]{:S(2)}) copy-start(bf16[4,512,512]{2,1,0:T(8,128)(2,1)} %values_far.1) | copy-start | bytes 6291460
  19.0 11.1 %copy-start.4 = (s32[4]{0:T(128)S(1)}, s32[4]{0:T(128)}, u32[]{:S(2)}) copy-start(s32[4]{0:T(128)} %lengths.1) | copy-start | bytes 52
  19.0 11.1 %copy-start.5 = (s32[4]{0:T(128)S(1)}, s32[4]{0:T(128)}, u32[]{:S(2)}) copy-start(s32[4]{0:T(128)} %accepted.1) | copy-start | bytes 52
  30.1 5.9 %copy-start.7 = (s32[4,24]{1,0:T(4,128)S(1)}, s32[4,24]{1,0:T(4,128)}, u32[]{:S(2)}) copy-start(s32[4,24]{1,0:T(4,128)} %parents.1) | copy-start | bytes 1156
  32.4 10.9 %all-to-all-start.2 = ((bf16[16,56,128]{2,1,0:T(8,128)(2,1)}), bf16[16,56,128]{2,1,0:T(8,128)(2,1)S(1)}, u32[]{:S(2)}, u32[]{:S(2)}) async-start(bf16[16,56,128]{2,1,0:T(8,128)(2,1)} %attend.1), calls=%async_computation.2 | async-start | bytes 458752 | tf_op jit(solution)/shard_map/all_to_all | solution.py:444
  35.9 7.3 %copy-start.3 = (f32[512]{0:T(512)S(1)}, f32[512]{0:T(512)}, u32[]{:S(2)}) copy-start(f32[512]{0:T(512)} %param.22) | copy-start | bytes 6148
  36.0 7.3 %copy-start.6 = (f32[8]{0:T(128)S(1)}, f32[8]{0:T(128)}, u32[]{:S(2)}) copy-start(f32[8]{0:T(128)} %param.21) | copy-start | bytes 100
  36.0 18.9 %copy-start.2 = (bf16[512,256]{1,0:T(8,128)(2,1)S(1)}, bf16[512,256]{1,0:T(8,128)(2,1)}, u32[]{:S(2)}) copy-start(bf16[512,256]{1,0:T(8,128)(2,1)} %w_output.1) | copy-start | bytes 786436
